TPU v7x, 32 devices: a whole 2x2x4 slice. The times are simulated.
32 devices in a mesh: ep: 8 (over z, core), tp: 4 (over y, x).
Axes of the slice: x: 2, y: 2, z: 4, core: 2. Of those that a mesh axis runs over, the one named last changes fastest.
Arguments:
- q_latent: bfloat16 [4096, 512], P('ep'), may hold values from -6 to 6
- kv_latent: bfloat16 [4096, 256], P('ep'), may hold values from -6 to 6
- rope_key: bfloat16 [4096, 32], P('ep'), may hold values from -400 to 400
- q_gain: bfloat16 [512], replicated, may hold values from 0.099609375 to 1.8984375
- kv_gain: bfloat16 [256], replicated, may hold values from 0.099609375 to 1.8984375
- w_q_nope: bfloat16 [512, 1024], P(None, 'tp'), may hold values from -0.25 to 0.25
- w_q_rope: bfloat16 [512, 512], P(None, 'tp'), may hold values from -0.25 to 0.25
- w_k_nope: bfloat16 [256, 1024], P(None, 'tp'), may hold values from -0.375 to 0.375
- w_value: bfloat16 [256, 1024], P(None, 'tp'), may hold values from -0.375 to 0.375
- w_out: bfloat16 [1024, 2048], P('tp'), may hold values from -5.375 to 5.375
- tokens_b: bfloat16 [1024, 2048], P('ep'), may hold values from -6 to 6
- norm_gain_b: bfloat16 [2048], replicated, may hold values from 0.099609375 to 1.8984375
- routes: int32 [1024, 2], P('ep'), may hold values from 0 to 7, all different within a row; in each aligned block of 128 rows (0 to 127, 128 to 255, ...) at most 48 rows name the same one
- route_logits: float32 [1024, 2], P('ep'), may hold values from -6 to 6
- w_gate: bfloat16 [8, 2048, 4096], P('ep', None, 'tp'), may hold values from -0.125 to 0.125
- w_up: bfloat16 [8, 2048, 4096], P('ep', None, 'tp'), may hold values from -0.125 to 0.125
- w_down: bfloat16 [8, 4096, 2048], P('ep', 'tp'), may hold values from -0.125 to 0.125
Outputs:
- mixer_out: bfloat16 [4096, 2048], P(('ep', 'tp'))
- expert_mix: bfloat16 [1024, 2048], P('ep', 'tp')
Inputs may be any that keep to these rules, and one draw needn't show every extreme that they name: `routes`: each row names two different experts. In each aligned block of 128 rows (the rows of one index of ep) no expert is named by more than 48 rows, and in every draw some expert is named by exactly 48 rows of some block.
All inputs are finite; a program needn't handle non-finite values.
Results may differ from a plain program's by a relative error of at most 0.022.
The roundings to bfloat16 on the way count: a program that leaves them out, or rounds other values in their place, can miss the bound.
Values may be sent and summed in bfloat16 or wider, within the bound.
A program may use at most 128 MiB of HBM per device.

v0:
```python
import jax
import jax.numpy as jnp
from jax import lax
from jax.sharding import PartitionSpec as P

NOPE = 64
ROPE = 32
VDIM = 64


EPSILON = 1e-06
FLOOR = -1e30


def rms_rows(values, gain):
    wide = values.astype(jnp.float32)
    scaled = wide * lax.rsqrt(jnp.mean(wide * wide, axis=-1, keepdims=True) + EPSILON)
    return (scaled * gain.astype(jnp.float32)).astype(jnp.bfloat16)


def rotate(values, places):
    half = values.shape[-1] // 2
    freqs = 10000.0 ** (-jnp.arange(half, dtype=jnp.float32) / half)
    angles = places.astype(jnp.float32)[:, None] * freqs[None, :]
    cosine = jnp.cos(angles)[:, None, :]
    sine = jnp.sin(angles)[:, None, :]
    first = values[..., :half]
    second = values[..., half:]
    return jnp.concatenate(
        [first * cosine - second * sine, first * sine + second * cosine], axis=-1
    )


def key_side(kv_piece, rope_piece, kv_gain, w_k_nope, w_value):
    count = kv_piece.shape[0]
    places = jnp.arange(count, dtype=jnp.int32)
    normed = rms_rows(kv_piece, kv_gain)
    k_nope = jnp.dot(normed, w_k_nope, preferred_element_type=jnp.float32).astype(jnp.bfloat16)
    values = jnp.dot(normed, w_value, preferred_element_type=jnp.float32).astype(jnp.bfloat16)
    k_rope = rotate(rope_piece.astype(jnp.float32)[:, None, :], places)[:, 0].astype(jnp.bfloat16)
    return (k_nope, values, k_rope)


def attend_block(carry, q_nope, q_rope, k_nope, values, k_rope):
    top, total_w, acc = carry
    heads = q_nope.shape[1]
    count = k_nope.shape[0]
    key_heads = k_nope.reshape(count, heads, NOPE)
    value_heads = values.reshape(count, heads, VDIM)
    scores = jnp.einsum("qhd,khd->hqk", q_nope, key_heads, preferred_element_type=jnp.float32)
    scores = scores + jnp.einsum("qhr,kr->hqk", q_rope, k_rope, preferred_element_type=jnp.float32)
    scores = scores * (NOPE + ROPE) ** (-0.5)
    new_top = jnp.maximum(top, jnp.max(scores, axis=-1))
    shrink = jnp.exp(top - new_top)
    weights = jnp.exp(scores - new_top[..., None])
    total_w = total_w * shrink + jnp.sum(weights, axis=-1)
    acc = acc * shrink[..., None] + jnp.einsum(
        "hqk,khd->hqd",
        weights.astype(jnp.bfloat16),
        value_heads,
        preferred_element_type=jnp.float32,
    )
    return (new_top, total_w, acc)


def attend(carry, q_nope, q_rope, k_nope, values, k_rope):
    count = k_nope.shape[0]
    span = 512

    def advance(state, pieces):
        return (attend_block(state, q_nope, q_rope, pieces[0], pieces[1], pieces[2]), None)

    blocks = (
        k_nope.reshape(count // span, span, k_nope.shape[1]),
        values.reshape(count // span, span, values.shape[1]),
        k_rope.reshape(count // span, span, k_rope.shape[1]),
    )
    carry, _ = lax.scan(advance, carry, blocks)
    return carry


def shards(
    q_latent,
    kv_latent,
    rope_key,
    q_gain,
    kv_gain,
    w_q_nope,
    w_q_rope,
    w_k_nope,
    w_value,
    w_out,
    tokens_b,
    norm_gain_b,
    routes,
    route_logits,
    w_gate,
    w_up,
    w_down,
):
    own_rows = q_latent.shape[0]
    heads = w_q_nope.shape[1] // NOPE
    offset = lax.axis_index("ep") * own_rows
    places = offset + jnp.arange(own_rows, dtype=jnp.int32)
    q_normed = rms_rows(q_latent, q_gain)
    q_nope = jnp.dot(q_normed, w_q_nope, preferred_element_type=jnp.float32).astype(jnp.bfloat16)
    q_nope = q_nope.reshape(own_rows, heads, NOPE)
    q_turn = jnp.dot(q_normed, w_q_rope, preferred_element_type=jnp.float32).reshape(
        own_rows, heads, ROPE
    )
    q_rope = rotate(q_turn, places).astype(jnp.bfloat16)
    start_carry = (
        jnp.full((heads, own_rows), FLOOR, jnp.float32),
        jnp.zeros((heads, own_rows), jnp.float32),
        jnp.zeros((heads, own_rows, VDIM), jnp.float32),
    )
    piece_keys, piece_values, piece_rotary = key_side(
        lax.all_gather(kv_latent, "ep", axis=0, tiled=True),
        lax.all_gather(rope_key, "ep", axis=0, tiled=True),
        kv_gain,
        w_k_nope,
        w_value,
    )
    top, total_w, acc = attend(start_carry, q_nope, q_rope, piece_keys, piece_values, piece_rotary)
    attended = (acc / total_w[..., None]).astype(jnp.bfloat16)
    attended = attended.transpose(1, 0, 2).reshape(own_rows, heads * VDIM)
    rows = attended
    mixer_out = lax.psum_scatter(
        jnp.dot(rows, w_out, preferred_element_type=jnp.float32).astype(jnp.bfloat16),
        "tp",
        scatter_dimension=0,
        tiled=True,
    )
    n_ep = lax.axis_size("ep")
    n_tp = lax.axis_size("tp")
    rows_b = tokens_b.shape[0]
    width = tokens_b.shape[1]
    room = 3 * rows_b // n_ep
    normed_b = rms_rows(tokens_b, norm_gain_b)
    weights_b = jax.nn.softmax(route_logits, axis=-1)
    flat = routes.reshape(-1)
    assigned = flat.shape[0]
    onehot = (flat[:, None] == jnp.arange(n_ep, dtype=jnp.int32)[None, :]).astype(jnp.int32)
    slot = jnp.sum((jnp.cumsum(onehot, axis=0) - 1) * onehot, axis=1)
    where = flat * room + slot
    table = (
        jnp.full((n_ep * room,), assigned, jnp.int32)
        .at[where]
        .set(jnp.arange(assigned, dtype=jnp.int32))
    )
    padded = jnp.concatenate([normed_b, jnp.zeros((1, width), jnp.bfloat16)], axis=0)
    share = width // n_tp
    narrow_rows = lax.dynamic_slice_in_dim(padded, lax.axis_index("tp") * share, share, 1)
    outgoing = narrow_rows[table // 2].reshape(n_ep, room, share)
    arrived = lax.all_to_all(outgoing, "ep", split_axis=0, concat_axis=0, tiled=True)
    sources, count, piece_width = arrived.shape
    rows = arrived.reshape(sources * count, piece_width)
    piece = lax.all_gather(rows, "tp", axis=1, tiled=True)
    gate_rows = w_gate[0]
    up_rows = w_up[0]
    gate = jnp.dot(piece, gate_rows, preferred_element_type=jnp.float32)
    up = jnp.dot(piece, up_rows, preferred_element_type=jnp.float32)
    hidden = (jax.nn.silu(gate) * up).astype(jnp.bfloat16)
    term = jnp.dot(hidden, w_down[0], preferred_element_type=jnp.float32)
    summed = lax.psum_scatter(
        term.astype(jnp.bfloat16), "tp", scatter_dimension=1, tiled=True
    ).astype(jnp.float32)
    finished = summed.astype(jnp.bfloat16).reshape(sources, count, summed.shape[1])
    back = lax.all_to_all(finished, "ep", split_axis=0, concat_axis=0, tiled=True)
    back = back.reshape(n_ep * room, back.shape[2])
    picked = back[where.reshape(rows_b, 2)].astype(jnp.float32)
    expert_mix = jnp.sum(picked * weights_b[:, :, None], axis=1).astype(jnp.bfloat16)
    return (mixer_out, expert_mix)


def solution(mesh):
    placed = (
        P("ep", None),
        P("ep", None),
        P("ep", None),
        P(),
        P(),
        P(None, "tp"),
        P(None, "tp"),
        P(None, "tp"),
        P(None, "tp"),
        P("tp", None),
        P("ep", None),
        P(),
        P("ep", None),
        P("ep", None),
        P("ep", None, "tp"),
        P("ep", None, "tp"),
        P("ep", "tp", None),
    )
    return jax.shard_map(
        shards,
        mesh=mesh,
        in_specs=placed,
        out_specs=(P(("ep", "tp"), None), P("ep", "tp")),
        check_vma=False,
    )
```

profile of v0, /device:TPU:1, one launch (start us, length us, event | category | flops | bytes accessed | tf_op | source)
XLA Modules:
  0.0 232.5 jit_solution(3116432101885813936)
XLA Ops:
  7.2 0.9 copy.27
  8.4 0.7 convert_element_type.106
  9.1 1.2 fusion.30
  11.6 1.4 scatter_custom_fusion
  13.1 1.2 fusion.32
  14.3 2.1 gather_fusion
  16.4 18.1 %all_to_all.10 = bf16[8,48,512]{2,1,0:T(8,128)(2,1)} all-to-all(bf16[8,48,512]{2,1,0:T(8,128)(2,1)S(1)} %bitcast.88), channel_id=1, replica_groups=mesh['ep'=8,'tp'=4] {'ep'}, dimensions={0} | all-to-all | bytes 786432 | tf_op jit(solution)/shard_map/all_to_all | solution.py:155
  34.6 0.7 all-gather.3.cloned.1.call-update
  35.4 14.9 %all_gather.10 = bf16[4096,32]{0,1:T(8,128)(2,1)S(1)} all-gather(bf16[512,32]{0,1:T(8,128)(2,1)S(1)} %copy-done.3), channel_id=1, replica_groups=mesh['ep'=8,'tp'=4] {'ep'}, dimensions={0}, use_global_device_ids=true | all-gather | bytes 294912 | tf_op jit(solution)/shard_map/all_gather | solution.py:119
  50.3 1.1 fusion.43
  53.1 11.2 %all-gather.5.cloned.1.call-done = bf16[384,2048]{1,0:T(8,128)(2,1)} async-done(((bf16[384,512]{1,0:T(8,128)(2,1)}), bf16[384,2048]{1,0:T(8,128)(2,1)}) %all-gather.5.cloned.1.call-update) | async-done | bytes 1572880 | tf_op jit(solution)/shard_map/all_gather | solution.py:158
  64.4 5.6 %fusion.20 = f32[384,1024]{1,0:T(8,128)} fusion(bf16[384,2048]{1,0:T(8,128)(2,1)} %all-gather.5.cloned.1.call-done, bf16[1,2048,1024]{2,1,0:T(8,128)(2,1)} %param.33), kind=kOutput, calls=%fused_computation.32 | convolution fusion | flops 1610612736 | bytes 7340032 | tf_op jit(solution)/shard_map/dot_general | solution.py:161
  70.0 9.3 %fusion.22 = bf16[384,2048]{1,0:T(8,128)(2,1)} fusion(bf16[1,1024,2048]{2,1,0:T(8,128)(2,1)} %param.35, f32[384,1024]{1,0:T(8,128)} %fusion.20, bf16[384,2048]{1,0:T(8,128)(2,1)} %all-gather.5.cloned.1.call-done, bf16[1,2048,1024]{2,1,0:T(8,128)(2,1)} %param.34), kind=kOutput, calls=%fused_computation.35 | convolution fusion | flops 3224371200 | bytes 13107200 | tf_op jit(solution)/shard_map/dot_general | solution.py:164
  79.6 16.1 %all-gather.3.cloned.1.call-done = bf16[4096,256]{1,0:T(8,128)(2,1)} async-done(((bf16[512,256]{1,0:T(8,128)(2,1)}), bf16[4096,256]{1,0:T(8,128)(2,1)}) %all-gather.3.cloned.1.call-update) | async-done | bytes 2097168 | tf_op jit(solution)/shard_map/all_gather | solution.py:118
  95.7 2.4 %fusion.13 = f32[4096]{0:T(1024)S(1)} fusion(bf16[4096,256]{1,0:T(8,128)(2,1)} %all-gather.3.cloned.1.call-done), kind=kLoop, calls=%fused_computation.25 | loop fusion | flops 3141632 | bytes 2113536 | tf_op jit(solution)/shard_map/reduce_sum | solution.py:17
  98.1 3.7 %convolution_convert_fusion.1 = bf16[4096,256]{1,0:T(8,128)(2,1)} fusion(bf16[256,256]{1,0:T(8,128)(2,1)S(1)} %copy-done.8, bf16[4096,256]{1,0:T(8,128)(2,1)} %all-gather.3.cloned.1.call-done, f32[256]{0:T(256)S(1)} %convert_element_type.92, f32[4096]{0:T(1024)S(1)} %add_rsqrt_fusion), kind=kOutput, calls=%fused_computation.24 | convolution fusion | flops 542113792 | bytes 4342784 | tf_op jit(solution)/shard_map/dot_general | solution.py:38
  101.8 2.0 convolution_convert_fusion
  103.8 85.5 %while.15 = (s32[]{:T(128)}, f32[4,512]{1,0:T(4,128)S(1)}, f32[4,512]{1,0:T(4,128)S(1)}, f32[4,512,64]{1,2,0:T(8,128)S(1)}, bf16[8,512,256]{2,1,0:T(8,128)(2,1)}...) while((s32[]{:T(128)}, f32[4,512]{1,0:T(4,128)S(1)}, ...), condition=%wide.region_5.6_spmd.clone, body=%wide.region_2.5_spmd.clone.sunk | while | flops 343287808 | bytes 25198728 | solution.py:78
  103.8 1.1 constant_dynamic-slice_fusion.3
  105.0 0.8 fusion.87
  105.8 2.7 %fusion.88 = (f32[4,512]{1,0:T(4,128)S(1)}, f32[4,512,512]{1,2,0:T(8,128)}) fusion(bf16[512,4,32]{0,2,1:T(8,128)(2,1)S(1)} %get-tuple-element.228, bf16[8,512,32]{1,2,0:T(8,128)(2,1)S(1)} %get-tuple-element.227, s32[]{:T(128)S(6)} %copy.43, f32[4,512,512]{2,1,0:T(8,128)S(1)} %fusion.87), kind=kOutput, calls=%fused_computation.101.clone.1 | convolution fusion | flops 70252544 | bytes 8560644 | tf_op jit(solution)/shard_map/while/body/eval_jaxpr/qhr,kr->hqk/dot_general | solution.py:51
  108.4 2.9 %fusion.89 = f32[4,512]{1,0:T(4,128)S(1)} fusion(f32[4,512,512]{1,2,0:T(8,128)} %get-tuple-element.195, f32[4,512]{1,0:T(4,128)S(1)} %select_maximum_fusion.2), kind=kLoop, calls=%fused_computation.7.clone.1 | loop fusion | flops 2095104 | bytes 4210688 | tf_op jit(solution)/shard_map/while/body/eval_jaxpr/reduce_sum | solution.py:56
  111.5 3.1 %fusion.91 = f32[4,512,64]{1,2,0:T(8,128)S(1)} fusion(bf16[512,4,64]{0,2,1:T(8,128)(2,1)S(1)} %bitcast.82, f32[4,512,512]{1,2,0:T(8,128)} %get-tuple-element.195, f32[4,512]{1,0:T(4,128)S(1)} %select_maximum_fusion.2, f32[4,512,64]{1,2,0:T(8,128)S(1)} %get-tuple-element.213, f32[4,512]{1,0:T(4,128)S(1)} %get-tuple-element.198, pred[]{:T(512)S(6)} %compare.6), kind=kOutput, calls=%fused_computation.10.clone.1 | convolution fusion | flops 136708096 | bytes 5521409 | tf_op jit(solution)/shard_map/while/body/eval_jaxpr/hqk,khd->hqd/dot_general | solution.py:57
  114.6 1.1 constant_dynamic-slice_fusion.3
  115.8 0.8 fusion.87
  116.6 2.7 %fusion.88 = (f32[4,512]{1,0:T(4,128)S(1)}, f32[4,512,512]{1,2,0:T(8,128)}) fusion(bf16[512,4,32]{0,2,1:T(8,128)(2,1)S(1)} %get-tuple-element.228, bf16[8,512,32]{1,2,0:T(8,128)(2,1)S(1)} %get-tuple-element.227, s32[]{:T(128)S(6)} %copy.43, f32[4,512,512]{2,1,0:T(8,128)S(1)} %fusion.87), kind=kOutput, calls=%fused_computation.101.clone.1 | convolution fusion | flops 70252544 | bytes 8560644 | tf_op jit(solution)/shard_map/while/body/eval_jaxpr/qhr,kr->hqk/dot_general | solution.py:51
  119.3 2.8 %fusion.89 = f32[4,512]{1,0:T(4,128)S(1)} fusion(f32[4,512,512]{1,2,0:T(8,128)} %get-tuple-element.195, f32[4,512]{1,0:T(4,128)S(1)} %select_maximum_fusion.2), kind=kLoop, calls=%fused_computation.7.clone.1 | loop fusion | flops 2095104 | bytes 4210688 | tf_op jit(solution)/shard_map/while/body/eval_jaxpr/reduce_sum | solution.py:56
  122.2 3.0 %fusion.91 = f32[4,512,64]{1,2,0:T(8,128)S(1)} fusion(bf16[512,4,64]{0,2,1:T(8,128)(2,1)S(1)} %bitcast.82, f32[4,512,512]{1,2,0:T(8,128)} %get-tuple-element.195, f32[4,512]{1,0:T(4,128)S(1)} %select_maximum_fusion.2, f32[4,512,64]{1,2,0:T(8,128)S(1)} %get-tuple-element.213, f32[4,512]{1,0:T(4,128)S(1)} %get-tuple-element.198, pred[]{:T(512)S(6)} %compare.6), kind=kOutput, calls=%fused_computation.10.clone.1 | convolution fusion | flops 136708096 | bytes 5521409 | tf_op jit(solution)/shard_map/while/body/eval_jaxpr/hqk,khd->hqd/dot_general | solution.py:57
  125.3 1.1 constant_dynamic-slice_fusion.3
  126.5 0.8 fusion.87
  127.3 2.7 %fusion.88 = (f32[4,512]{1,0:T(4,128)S(1)}, f32[4,512,512]{1,2,0:T(8,128)}) fusion(bf16[512,4,32]{0,2,1:T(8,128)(2,1)S(1)} %get-tuple-element.228, bf16[8,512,32]{1,2,0:T(8,128)(2,1)S(1)} %get-tuple-element.227, s32[]{:T(128)S(6)} %copy.43, f32[4,512,512]{2,1,0:T(8,128)S(1)} %fusion.87), kind=kOutput, calls=%fused_computation.101.clone.1 | convolution fusion | flops 70252544 | bytes 8560644 | tf_op jit(solution)/shard_map/while/body/eval_jaxpr/qhr,kr->hqk/dot_general | solution.py:51
  130.0 2.8 %fusion.89 = f32[4,512]{1,0:T(4,128)S(1)} fusion(f32[4,512,512]{1,2,0:T(8,128)} %get-tuple-element.195, f32[4,512]{1,0:T(4,128)S(1)} %select_maximum_fusion.2), kind=kLoop, calls=%fused_computation.7.clone.1 | loop fusion | flops 2095104 | bytes 4210688 | tf_op jit(solution)/shard_map/while/body/eval_jaxpr/reduce_sum | solution.py:56
  132.9 3.0 %fusion.91 = f32[4,512,64]{1,2,0:T(8,128)S(1)} fusion(bf16[512,4,64]{0,2,1:T(8,128)(2,1)S(1)} %bitcast.82, f32[4,512,512]{1,2,0:T(8,128)} %get-tuple-element.195, f32[4,512]{1,0:T(4,128)S(1)} %select_maximum_fusion.2, f32[4,512,64]{1,2,0:T(8,128)S(1)} %get-tuple-element.213, f32[4,512]{1,0:T(4,128)S(1)} %get-tuple-element.198, pred[]{:T(512)S(6)} %compare.6), kind=kOutput, calls=%fused_computation.10.clone.1 | convolution fusion | flops 136708096 | bytes 5521409 | tf_op jit(solution)/shard_map/while/body/eval_jaxpr/hqk,khd->hqd/dot_general | solution.py:57
  136.0 1.1 constant_dynamic-slice_fusion.3
  137.2 0.8 fusion.87
  137.9 2.7 %fusion.88 = (f32[4,512]{1,0:T(4,128)S(1)}, f32[4,512,512]{1,2,0:T(8,128)}) fusion(bf16[512,4,32]{0,2,1:T(8,128)(2,1)S(1)} %get-tuple-element.228, bf16[8,512,32]{1,2,0:T(8,128)(2,1)S(1)} %get-tuple-element.227, s32[]{:T(128)S(6)} %copy.43, f32[4,512,512]{2,1,0:T(8,128)S(1)} %fusion.87), kind=kOutput, calls=%fused_computation.101.clone.1 | convolution fusion | flops 70252544 | bytes 8560644 | tf_op jit(solution)/shard_map/while/body/eval_jaxpr/qhr,kr->hqk/dot_general | solution.py:51
  140.6 2.8 %fusion.89 = f32[4,512]{1,0:T(4,128)S(1)} fusion(f32[4,512,512]{1,2,0:T(8,128)} %get-tuple-element.195, f32[4,512]{1,0:T(4,128)S(1)} %select_maximum_fusion.2), kind=kLoop, calls=%fused_computation.7.clone.1 | loop fusion | flops 2095104 | bytes 4210688 | tf_op jit(solution)/shard_map/while/body/eval_jaxpr/reduce_sum | solution.py:56
  143.6 3.0 %fusion.91 = f32[4,512,64]{1,2,0:T(8,128)S(1)} fusion(bf16[512,4,64]{0,2,1:T(8,128)(2,1)S(1)} %bitcast.82, f32[4,512,512]{1,2,0:T(8,128)} %get-tuple-element.195, f32[4,512]{1,0:T(4,128)S(1)} %select_maximum_fusion.2, f32[4,512,64]{1,2,0:T(8,128)S(1)} %get-tuple-element.213, f32[4,512]{1,0:T(4,128)S(1)} %get-tuple-element.198, pred[]{:T(512)S(6)} %compare.6), kind=kOutput, calls=%fused_computation.10.clone.1 | convolution fusion | flops 136708096 | bytes 5521409 | tf_op jit(solution)/shard_map/while/body/eval_jaxpr/hqk,khd->hqd/dot_general | solution.py:57
  146.6 1.1 constant_dynamic-slice_fusion.3
  147.8 0.8 fusion.87
  148.6 2.7 %fusion.88 = (f32[4,512]{1,0:T(4,128)S(1)}, f32[4,512,512]{1,2,0:T(8,128)}) fusion(bf16[512,4,32]{0,2,1:T(8,128)(2,1)S(1)} %get-tuple-element.228, bf16[8,512,32]{1,2,0:T(8,128)(2,1)S(1)} %get-tuple-element.227, s32[]{:T(128)S(6)} %copy.43, f32[4,512,512]{2,1,0:T(8,128)S(1)} %fusion.87), kind=kOutput, calls=%fused_computation.101.clone.1 | convolution fusion | flops 70252544 | bytes 8560644 | tf_op jit(solution)/shard_map/while/body/eval_jaxpr/qhr,kr->hqk/dot_general | solution.py:51
  151.3 2.8 %fusion.89 = f32[4,512]{1,0:T(4,128)S(1)} fusion(f32[4,512,512]{1,2,0:T(8,128)} %get-tuple-element.195, f32[4,512]{1,0:T(4,128)S(1)} %select_maximum_fusion.2), kind=kLoop, calls=%fused_computation.7.clone.1 | loop fusion | flops 2095104 | bytes 4210688 | tf_op jit(solution)/shard_map/while/body/eval_jaxpr/reduce_sum | solution.py:56
  154.2 3.0 %fusion.91 = f32[4,512,64]{1,2,0:T(8,128)S(1)} fusion(bf16[512,4,64]{0,2,1:T(8,128)(2,1)S(1)} %bitcast.82, f32[4,512,512]{1,2,0:T(8,128)} %get-tuple-element.195, f32[4,512]{1,0:T(4,128)S(1)} %select_maximum_fusion.2, f32[4,512,64]{1,2,0:T(8,128)S(1)} %get-tuple-element.213, f32[4,512]{1,0:T(4,128)S(1)} %get-tuple-element.198, pred[]{:T(512)S(6)} %compare.6), kind=kOutput, calls=%fused_computation.10.clone.1 | convolution fusion | flops 136708096 | bytes 5521409 | tf_op jit(solution)/shard_map/while/body/eval_jaxpr/hqk,khd->hqd/dot_general | solution.py:57
  157.3 1.1 constant_dynamic-slice_fusion.3
  158.5 0.8 fusion.87
  159.3 2.7 %fusion.88 = (f32[4,512]{1,0:T(4,128)S(1)}, f32[4,512,512]{1,2,0:T(8,128)}) fusion(bf16[512,4,32]{0,2,1:T(8,128)(2,1)S(1)} %get-tuple-element.228, bf16[8,512,32]{1,2,0:T(8,128)(2,1)S(1)} %get-tuple-element.227, s32[]{:T(128)S(6)} %copy.43, f32[4,512,512]{2,1,0:T(8,128)S(1)} %fusion.87), kind=kOutput, calls=%fused_computation.101.clone.1 | convolution fusion | flops 70252544 | bytes 8560644 | tf_op jit(solution)/shard_map/while/body/eval_jaxpr/qhr,kr->hqk/dot_general | solution.py:51
  161.9 2.8 %fusion.89 = f32[4,512]{1,0:T(4,128)S(1)} fusion(f32[4,512,512]{1,2,0:T(8,128)} %get-tuple-element.195, f32[4,512]{1,0:T(4,128)S(1)} %select_maximum_fusion.2), kind=kLoop, calls=%fused_computation.7.clone.1 | loop fusion | flops 2095104 | bytes 4210688 | tf_op jit(solution)/shard_map/while/body/eval_jaxpr/reduce_sum | solution.py:56
  164.9 3.0 %fusion.91 = f32[4,512,64]{1,2,0:T(8,128)S(1)} fusion(bf16[512,4,64]{0,2,1:T(8,128)(2,1)S(1)} %bitcast.82, f32[4,512,512]{1,2,0:T(8,128)} %get-tuple-element.195, f32[4,512]{1,0:T(4,128)S(1)} %select_maximum_fusion.2, f32[4,512,64]{1,2,0:T(8,128)S(1)} %get-tuple-element.213, f32[4,512]{1,0:T(4,128)S(1)} %get-tuple-element.198, pred[]{:T(512)S(6)} %compare.6), kind=kOutput, calls=%fused_computation.10.clone.1 | convolution fusion | flops 136708096 | bytes 5521409 | tf_op jit(solution)/shard_map/while/body/eval_jaxpr/hqk,khd->hqd/dot_general | solution.py:57
  167.9 1.1 constant_dynamic-slice_fusion.3
  169.2 0.8 fusion.87
  169.9 2.7 %fusion.88 = (f32[4,512]{1,0:T(4,128)S(1)}, f32[4,512,512]{1,2,0:T(8,128)}) fusion(bf16[512,4,32]{0,2,1:T(8,128)(2,1)S(1)} %get-tuple-element.228, bf16[8,512,32]{1,2,0:T(8,128)(2,1)S(1)} %get-tuple-element.227, s32[]{:T(128)S(6)} %copy.43, f32[4,512,512]{2,1,0:T(8,128)S(1)} %fusion.87), kind=kOutput, calls=%fused_computation.101.clone.1 | convolution fusion | flops 70252544 | bytes 8560644 | tf_op jit(solution)/shard_map/while/body/eval_jaxpr/qhr,kr->hqk/dot_general | solution.py:51
  172.6 2.8 %fusion.89 = f32[4,512]{1,0:T(4,128)S(1)} fusion(f32[4,512,512]{1,2,0:T(8,128)} %get-tuple-element.195, f32[4,512]{1,0:T(4,128)S(1)} %select_maximum_fusion.2), kind=kLoop, calls=%fused_computation.7.clone.1 | loop fusion | flops 2095104 | bytes 4210688 | tf_op jit(solution)/shard_map/while/body/eval_jaxpr/reduce_sum | solution.py:56
  175.5 3.0 %fusion.91 = f32[4,512,64]{1,2,0:T(8,128)S(1)} fusion(bf16[512,4,64]{0,2,1:T(8,128)(2,1)S(1)} %bitcast.82, f32[4,512,512]{1,2,0:T(8,128)} %get-tuple-element.195, f32[4,512]{1,0:T(4,128)S(1)} %select_maximum_fusion.2, f32[4,512,64]{1,2,0:T(8,128)S(1)} %get-tuple-element.213, f32[4,512]{1,0:T(4,128)S(1)} %get-tuple-element.198, pred[]{:T(512)S(6)} %compare.6), kind=kOutput, calls=%fused_computation.10.clone.1 | convolution fusion | flops 136708096 | bytes 5521409 | tf_op jit(solution)/shard_map/while/body/eval_jaxpr/hqk,khd->hqd/dot_general | solution.py:57
  178.6 1.1 constant_dynamic-slice_fusion.3
  179.8 0.8 fusion.87
  180.6 2.7 %fusion.88 = (f32[4,512]{1,0:T(4,128)S(1)}, f32[4,512,512]{1,2,0:T(8,128)}) fusion(bf16[512,4,32]{0,2,1:T(8,128)(2,1)S(1)} %get-tuple-element.228, bf16[8,512,32]{1,2,0:T(8,128)(2,1)S(1)} %get-tuple-element.227, s32[]{:T(128)S(6)} %copy.43, f32[4,512,512]{2,1,0:T(8,128)S(1)} %fusion.87), kind=kOutput, calls=%fused_computation.101.clone.1 | convolution fusion | flops 70252544 | bytes 8560644 | tf_op jit(solution)/shard_map/while/body/eval_jaxpr/qhr,kr->hqk/dot_general | solution.py:51
  183.3 2.8 %fusion.89 = f32[4,512]{1,0:T(4,128)S(1)} fusion(f32[4,512,512]{1,2,0:T(8,128)} %get-tuple-element.195, f32[4,512]{1,0:T(4,128)S(1)} %select_maximum_fusion.2), kind=kLoop, calls=%fused_computation.7.clone.1 | loop fusion | flops 2095104 | bytes 4210688 | tf_op jit(solution)/shard_map/while/body/eval_jaxpr/reduce_sum | solution.py:56
  186.2 3.0 %fusion.91 = f32[4,512,64]{1,2,0:T(8,128)S(1)} fusion(bf16[512,4,64]{0,2,1:T(8,128)(2,1)S(1)} %bitcast.82, f32[4,512,512]{1,2,0:T(8,128)} %get-tuple-element.195, f32[4,512]{1,0:T(4,128)S(1)} %select_maximum_fusion.2, f32[4,512,64]{1,2,0:T(8,128)S(1)} %get-tuple-element.213, f32[4,512]{1,0:T(4,128)S(1)} %get-tuple-element.198, pred[]{:T(512)S(6)} %compare.6), kind=kOutput, calls=%fused_computation.10.clone.1 | convolution fusion | flops 136708096 | bytes 5521409 | tf_op jit(solution)/shard_map/while/body/eval_jaxpr/hqk,khd->hqd/dot_general | solution.py:57
  189.3 2.1 convolution_convert_fusion.2
  191.5 3.8 %all-to-all-start.1 = ((bf16[8,48,512]{2,1,0:T(8,128)(2,1)}), bf16[8,48,512]{2,1,0:T(8,128)(2,1)S(1)}, u32[]{:S(2)}, u32[]{:S(2)}) async-start(bf16[8,48,512]{2,1,0:T(8,128)(2,1)} %bitcast.93), calls=%async_computation.3 | async-start | bytes 786432 | tf_op jit(solution)/shard_map/all_to_all | solution.py:169
  195.6 11.1 %all-to-all-done.1 = bf16[8,48,512]{2,1,0:T(8,128)(2,1)S(1)} async-done(((bf16[8,48,512]{2,1,0:T(8,128)(2,1)}), bf16[8,48,512]{2,1,0:T(8,128)(2,1)S(1)}, u32[]{:S(2)}, u32[]{:S(2)}) %all-to-all-start.1) | async-done | bytes 393248 | tf_op jit(solution)/shard_map/all_to_all | solution.py:169
  206.7 1.2 gather_fusion.1
  208.2 1.4 multiply_reduce_fusion
  209.5 16.4 %reduce-scatter.3.cloned.1.call-done = bf16[128,2048]{1,0:T(8,128)(2,1)} async-done(((bf16[512,2048]{1,0:T(8,128)(2,1)}), bf16[128,2048]{1,0:T(8,128)(2,1)}) %reduce-scatter.3.cloned.1.call-update) | async-done | bytes 524304 | tf_op jit(solution)/shard_map/reduce_scatter | solution.py:128
  (115 shorter events, 6.8 us)
Async XLA Ops:
  7.2 182.2 %copy-start = (bf16[256,2048]{1,0:T(8,128)(2,1)S(1)}, bf16[256,2048]{1,0:T(8,128)(2,1)}, u32[]{:S(2)}) copy-start(bf16[256,2048]{1,0:T(8,128)(2,1)} %param.28) | copy-start | bytes 3145732
  7.2 28.2 %copy-start.3 = (bf16[512,32]{0,1:T(8,128)(2,1)S(1)}, bf16[512,32]{0,1:T(8,128)(2,1)}, u32[]{:S(2)}) copy-start(bf16[512,32]{0,1:T(8,128)(2,1)} %param.21) | copy-start | bytes 98308
  7.2 57.2 %all-gather.5.cloned.1.call-start = ((), (), s32[]{:S(2)}) async-start(), calls=%async_computation.6 | async-start | bytes 1966080 | tf_op jit(solution)/shard_map/all_gather | solution.py:158
  13.0 38.5 %copy-start.10 = (bf16[256]{0:T(256)(128)(2,1)S(1)}, bf16[256]{0:T(256)(128)(2,1)}, u32[]{:S(2)}) copy-start(bf16[256]{0:T(256)(128)(2,1)} %param.23) | copy-start | bytes 1540
  13.0 38.5 %copy-start.5 = (bf16[512]{0:T(512)(128)(2,1)S(1)}, bf16[512]{0:T(512)(128)(2,1)}, u32[]{:S(2)}) copy-start(bf16[512]{0:T(512)(128)(2,1)} %param.22) | copy-start | bytes 3076
  14.3 37.4 %copy-start.2 = (bf16[512,512]{1,0:T(8,128)(2,1)S(1)}, bf16[512,512]{1,0:T(8,128)(2,1)}, u32[]{:S(2)}) copy-start(bf16[512,512]{1,0:T(8,128)(2,1)} %param.19) | copy-start | bytes 1572868
  14.3 37.8 %copy-start.7 = (bf16[512,128]{1,0:T(8,128)(2,1)S(1)}, bf16[512,128]{1,0:T(8,128)(2,1)}, u32[]{:S(2)}) copy-start(bf16[512,128]{1,0:T(8,128)(2,1)} %param.25) | copy-start | bytes 393220
  16.4 36.3 %copy-start.6 = (bf16[512,256]{1,0:T(8,128)(2,1)S(1)}, bf16[512,256]{1,0:T(8,128)(2,1)}, u32[]{:S(2)}) copy-start(bf16[512,256]{1,0:T(8,128)(2,1)} %param.24) | copy-start | bytes 786436
  34.5 61.2 %all-gather.3.cloned.1.call-start = ((), (), s32[]{:S(2)}) async-start(), calls=%async_computation.4 | async-start | bytes 2359296 | tf_op jit(solution)/shard_map/all_gather | solution.py:118
  35.3 156.2 %reduce-scatter.5.cloned.1.call-start = ((), (), s32[]{:S(2)}) async-start(), calls=%async_computation.7 | async-start | bytes 1966080 | tf_op jit(solution)/shard_map/reduce_scatter | solution.py:165
  70.0 28.1 %copy-start.8 = (bf16[256,256]{1,0:T(8,128)(2,1)S(1)}, bf16[256,256]{1,0:T(8,128)(2,1)}, u32[]{:S(2)}) copy-start(bf16[256,256]{1,0:T(8,128)(2,1)} %param.26) | copy-start | bytes 393220
  79.3 22.5 %copy-start.9 = (bf16[256,256]{1,0:T(8,128)(2,1)S(1)}, bf16[256,256]{1,0:T(8,128)(2,1)}, u32[]{:S(2)}) copy-start(bf16[256,256]{1,0:T(8,128)(2,1)} %param.27) | copy-start | bytes 393220
  79.3 146.6 %reduce-scatter.3.cloned.1.call-start = ((), (), s32[]{:S(2)}) async-start(), calls=%async_computation.5 | async-start | bytes 2621440 | tf_op jit(solution)/shard_map/reduce_scatter | solution.py:128
  95.7 6.1 %copy-start.1 = (bf16[4096,256]{1,0:T(8,128)(2,1)S(1)}, bf16[4096,256]{1,0:T(8,128)(2,1)}, u32[]{:S(2)}) copy-start(bf16[4096,256]{1,0:T(8,128)(2,1)} %all-gather.3.cloned.1.call-done) | copy-start | bytes 6291460
  189.3 6.2 %copy-start.4 = (f32[128,2]{0,1:T(2,128)S(1)}, f32[128,2]{0,1:T(2,128)}, u32[]{:S(2)}) copy-start(f32[128,2]{0,1:T(2,128)} %param.32) | copy-start | bytes 3076
  191.5 15.2 %all-to-all-start.1 = ((bf16[8,48,512]{2,1,0:T(8,128)(2,1)}), bf16[8,48,512]{2,1,0:T(8,128)(2,1)S(1)}, u32[]{:S(2)}, u32[]{:S(2)}) async-start(bf16[8,48,512]{2,1,0:T(8,128)(2,1)} %bitcast.93), calls=%async_computation.3 | async-start | bytes 786432 | tf_op jit(solution)/shard_map/all_to_all | solution.py:169
Sparse Core Ops, SparseCore 0:
  34.6 29.6 all-gather.4
  66.0 29.6 all-gather.2
  98.7 29.9 reduce-scatter.4
  191.6 34.3 reduce-scatter.2
where the time goes:
time: 234 us; the launch traced here: 232 us
  matrix products  75.3 us (32%)
  waiting for transfers between devices  55.6 us (24%)
  blocking collectives  33 us (14%)
  other arithmetic  31.9 us (14%)
  local copies, waits for them, and re-layouts  17.9 us (8%)
  between operations  14.2 us (6%)
  starting transfers between devices  4.11 us (2%)
    dot_general x8, matrix products, attend_block(): jnp.einsum('hqk,khd->hqd', weights.astype(jnp.bfloat16), value_heads, pre...  24.4 us
    reduce_sum x8, other arithmetic, attend_block(): total_w = total_w * shrink + jnp.sum(weights, axis=-1)  22.2 us
    dot_general x8, matrix products, attend_block(): jnp.einsum('qhr,kr->hqk', q_rope, k_rope, preferred_element_type=jnp.floa...  21.3 us
    all_to_all x1, blocking collectives, shards(): lax.all_to_all(outgoing, 'ep', split_axis=0, concat_axis=0, tiled=True)  18.1 us
    reduce_scatter x1, waiting for transfers between devices, shards(): lax.psum_scatter(jnp.dot(rows, w_out, preferred_element_type=jnp.float32)...  16.4 us
    all_gather x1, waiting for transfers between devices, shards(): lax.all_gather(kv_latent, 'ep', axis=0, tiled=True)  16.1 us
    all_gather x1, blocking collectives, shards(): lax.all_gather(rope_key, 'ep', axis=0, tiled=True)  14.9 us
    all_gather x1, waiting for transfers between devices, shards(): piece = lax.all_gather(rows, 'tp', axis=1, tiled=True)  11.2 us
  transfers between devices with their start and end apart: 5, of which 4 were waited for; matrix products, arithmetic and copies ran while one was open for 50% of the time, Pallas kernels for 0%

commit v1 on v0

v1 whole, which is shorter than its diff:
```python
import functools
import math

import jax
import jax.numpy as jnp
from jax import lax
from jax.experimental import pallas as pl
from jax.experimental.pallas import tpu as pltpu
from jax.sharding import PartitionSpec as P

NOPE = 64
ROPE = 32
VDIM = 64
LANES = 128
EPSILON = 1e-06
BF = jnp.bfloat16
F32 = jnp.float32


def rms_rows(values, gain):
    wide = values.astype(F32)
    scaled = wide * lax.rsqrt(jnp.mean(wide * wide, axis=-1, keepdims=True) + EPSILON)
    return (scaled * gain.astype(F32)).astype(BF)


def angle_tables(places):
    half = ROPE // 2
    freqs = 10000.0 ** (-jnp.arange(half, dtype=F32) / half)
    angles = places.astype(F32)[:, None] * freqs[None, :]
    return jnp.cos(angles), jnp.sin(angles)


def attention_kernel(heads, q_ref, kv_ref, w_ref, out_ref, k_buf, v_buf):
    keys = kv_ref.shape[0]
    rows = q_ref.shape[1]
    scale = (NOPE + ROPE) ** (-0.5) * math.log2(math.e)
    chunk = 512
    q_block = min(256, rows)
    k_block = 1024
    wide = heads * LANES

    def project(c, _):
        here = pl.ds(pl.multiple_of(c * chunk, chunk), chunk)
        up = jnp.dot(kv_ref[here, :], w_ref[...], preferred_element_type=F32)
        lane = lax.broadcasted_iota(jnp.int32, (chunk, LANES), 1)
        for h in range(heads):
            k_buf[h, here, :] = up[:, h * LANES : (h + 1) * LANES].astype(BF)
            v = up[:, wide + h * LANES : wide + (h + 1) * LANES]
            v_buf[h, here, :] = jnp.where(lane < VDIM, v, 1.0).astype(BF)
        return 0

    lax.fori_loop(0, keys // chunk, project, 0)

    def attend(step, _):
        h = step // (rows // q_block)
        b = step % (rows // q_block)
        here = pl.ds(pl.multiple_of(b * q_block, q_block), q_block)
        q = q_ref[h, here, :]
        top = jnp.full((q_block, 1), -jnp.inf, F32)
        acc = jnp.zeros((q_block, LANES), F32)
        for j in range(keys // k_block):
            at = slice(j * k_block, (j + 1) * k_block)
            s = lax.dot_general(
                q, k_buf[h, at, :], (((1,), (1,)), ((), ())), preferred_element_type=F32
            )
            new_top = jnp.maximum(top, jnp.max(s, axis=-1, keepdims=True))
            p = jnp.exp2((s - new_top) * scale).astype(BF)
            pv = jnp.dot(p, v_buf[h, at, :], preferred_element_type=F32)
            if j == 0:
                acc = pv
            else:
                acc = acc * jnp.exp2((top - new_top) * scale) + pv
            top = new_top
        out_ref[h, here, :] = (acc[:, :VDIM] / acc[:, VDIM : VDIM + 1]).astype(BF)
        return 0

    lax.fori_loop(0, heads * (rows // q_block), attend, 0)


def attention(q, kv, w):
    heads, rows, _ = q.shape
    keys = kv.shape[0]
    flops = 4 * heads * rows * keys * 256
    return pl.pallas_call(
        functools.partial(attention_kernel, heads),
        out_shape=jax.ShapeDtypeStruct((heads, rows, VDIM), BF),
        in_specs=[pl.BlockSpec(memory_space=pltpu.VMEM)] * 3,
        out_specs=pl.BlockSpec(memory_space=pltpu.VMEM),
        scratch_shapes=[
            pltpu.VMEM((heads, keys, LANES), BF),
            pltpu.VMEM((heads, keys, LANES), BF),
        ],
        compiler_params=pltpu.CompilerParams(vmem_limit_bytes=48 * 1024 * 1024),
        cost_estimate=pl.CostEstimate(
            flops=flops, bytes_accessed=8 * 1024 * 1024, transcendentals=heads * rows * keys
        ),
        name="attention",
    )(q, kv, w)


def lay_heads(weights, heads, width, offset):
    depth = weights.shape[0]
    split = weights.reshape(depth, heads, width)
    return jnp.pad(split, ((0, 0), (0, 0), (offset, LANES - width - offset)))


def shards(
    q_latent,
    kv_latent,
    rope_key,
    q_gain,
    kv_gain,
    w_q_nope,
    w_q_rope,
    w_k_nope,
    w_value,
    w_out,
    tokens_b,
    norm_gain_b,
    routes,
    route_logits,
    w_gate,
    w_up,
    w_down,
):
    n_ep = lax.axis_size("ep")
    n_tp = lax.axis_size("tp")
    e_at = lax.axis_index("ep")
    t_at = lax.axis_index("tp")
    own_rows = q_latent.shape[0]
    heads = w_q_nope.shape[1] // NOPE
    rows_b = tokens_b.shape[0]
    width = tokens_b.shape[1]
    half = ROPE // 2

    part = own_rows // n_tp
    kv_part = lax.dynamic_slice_in_dim(kv_latent, t_at * part, part, 0)
    rope_part = lax.dynamic_slice_in_dim(rope_key, t_at * part, part, 0).astype(F32)
    places = e_at * own_rows + t_at * part + jnp.arange(part, dtype=jnp.int32)
    cosine, sine = angle_tables(places)
    first, second = rope_part[:, :half], rope_part[:, half:]
    sent = jnp.concatenate(
        [
            rms_rows(kv_part, kv_gain),
            (first * cosine - second * sine).astype(BF),
            (first * sine + second * cosine).astype(BF),
        ],
        axis=1,
    )
    kv_all = lax.all_gather(sent, ("ep", "tp"), axis=0, tiled=True)

    part_b = rows_b // n_tp
    tok_part = lax.dynamic_slice_in_dim(tokens_b, t_at * part_b, part_b, 0)
    route_part = lax.dynamic_slice_in_dim(routes, t_at * part_b, part_b, 0)
    logit_part = lax.dynamic_slice_in_dim(route_logits, t_at * part_b, part_b, 0)
    weights_b = jax.nn.softmax(logit_part, axis=-1)
    high = weights_b.astype(BF)
    low = (weights_b - high.astype(F32)).astype(BF)
    extra = jnp.concatenate(
        [route_part.astype(BF), high, low, jnp.zeros((part_b, LANES - 6), BF)], axis=1
    )
    sent_b = jnp.concatenate([rms_rows(tok_part, norm_gain_b), extra], axis=1)
    tok_all = lax.all_gather(sent_b, ("ep", "tp"), axis=0, tiled=True)

    q_normed = rms_rows(q_latent, q_gain)
    w_nope = lay_heads(w_q_nope, heads, NOPE, 0)
    w_rope = lay_heads(w_q_rope, heads, ROPE, NOPE)
    turn = w_q_rope.reshape(-1, heads, ROPE)
    turned = jnp.concatenate([-turn[..., half:], turn[..., :half]], axis=-1)
    w_turned = jnp.pad(turned, ((0, 0), (0, 0), (NOPE, LANES - NOPE - ROPE)))
    cos_q, sin_q = angle_tables(e_at * own_rows + jnp.arange(own_rows, dtype=jnp.int32))
    ones = jnp.ones((own_rows, NOPE), F32)
    tail = jnp.zeros((own_rows, LANES - NOPE - ROPE), F32)
    cos_row = jnp.concatenate([ones, cos_q, cos_q, tail], axis=1)
    sin_row = jnp.concatenate([0.0 * ones, sin_q, sin_q, tail], axis=1)
    plain = jnp.einsum("rd,dhl->hrl", q_normed, w_nope + w_rope, preferred_element_type=F32)
    swapped = jnp.einsum("rd,dhl->hrl", q_normed, w_turned, preferred_element_type=F32)
    q = (plain * cos_row + swapped * sin_row).astype(BF)

    place = jnp.pad(jnp.eye(ROPE, dtype=BF), ((0, 0), (NOPE, LANES - NOPE - ROPE)))
    place = jnp.broadcast_to(place[:, None, :], (ROPE, heads, LANES))
    w_keys = jnp.concatenate([lay_heads(w_k_nope, heads, NOPE, 0), place], axis=0)
    w_vals = jnp.pad(lay_heads(w_value, heads, VDIM, 0), ((0, ROPE), (0, 0), (0, 0)))
    w_kv = jnp.concatenate(
        [w_keys.reshape(-1, heads * LANES), w_vals.reshape(-1, heads * LANES)], axis=1
    )
    attended = attention(q, kv_all, w_kv)
    attended = attended.transpose(1, 0, 2).reshape(own_rows, heads * VDIM)
    mixer_out = lax.psum_scatter(
        jnp.dot(attended, w_out, preferred_element_type=F32).astype(BF),
        "tp",
        scatter_dimension=0,
        tiled=True,
    )

    room = 3 * rows_b // n_ep
    total_b = tok_all.shape[0]
    info = tok_all[:, width : width + LANES].astype(F32)
    me = e_at.astype(F32)
    hit_0 = (info[:, 0] == me).astype(F32)
    hit_1 = (info[:, 1] == me).astype(F32)
    hit = hit_0 + hit_1
    weight = hit_0 * (info[:, 2] + info[:, 4]) + hit_1 * (info[:, 3] + info[:, 5])
    order = jnp.arange(rows_b)
    before = (order[:, None] < order[None, :]).astype(BF)
    slot = jnp.dot(hit.reshape(n_ep, rows_b).astype(BF), before, preferred_element_type=F32)
    row = slot + (jnp.arange(n_ep, dtype=F32) * room)[:, None]
    row = jnp.where(hit > 0, row.reshape(total_b), -1.0)
    index = jnp.arange(n_ep * room, dtype=F32)
    chosen = index[:, None] == row[None, :]
    pick = chosen.astype(BF)
    row_weight = jnp.sum(jnp.where(chosen, weight[None, :], 0.0), axis=1, keepdims=True)
    piece = jnp.dot(pick, tok_all[:, :width], preferred_element_type=F32).astype(BF)
    gate = jnp.dot(piece, w_gate[0], preferred_element_type=F32)
    up = jnp.dot(piece, w_up[0], preferred_element_type=F32)
    hidden = (jax.nn.silu(gate) * up).astype(BF)
    term = jnp.dot(hidden, w_down[0], preferred_element_type=F32)
    scaled = (term * row_weight).astype(BF)
    share = width // n_tp
    spread = jnp.einsum(
        "reb,rjc->ejbc",
        pick.reshape(n_ep * room, n_ep, rows_b),
        scaled.reshape(n_ep * room, n_tp, share),
        preferred_element_type=F32,
    ).astype(BF)
    expert_mix = lax.psum_scatter(
        spread.reshape(n_ep * n_tp * rows_b, share), ("ep", "tp"), scatter_dimension=0, tiled=True
    )
    return (mixer_out, expert_mix)


def solution(mesh):
    placed = (
        P("ep", None),
        P("ep", None),
        P("ep", None),
        P(),
        P(),
        P(None, "tp"),
        P(None, "tp"),
        P(None, "tp"),
        P(None, "tp"),
        P("tp", None),
        P("ep", None),
        P(),
        P("ep", None),
        P("ep", None),
        P("ep", None, "tp"),
        P("ep", None, "tp"),
        P("ep", "tp", None),
    )
    return jax.shard_map(
        shards,
        mesh=mesh,
        in_specs=placed,
        out_specs=(P(("ep", "tp"), None), P("ep", "tp")),
        check_vma=False,
    )
```

time: 234 us -> 328 us (1.40); the launches traced: 232 us -> 323 us
  waiting for transfers between devices: 55.6 us -> 241 us
  matrix products: 75.3 us -> 19.5 us
  blocking collectives: 33 us -> 0 us
  Pallas kernels: 0 us -> 21.7 us
  other arithmetic: 31.9 us -> 13.3 us
  local copies, waits for them, and re-layouts: 17.9 us -> 12.7 us
  starting transfers between devices: 4.11 us -> 0.34 us
    reduce_scatter x2, waiting for transfers between devices: 16.5 us -> 153 us  [the longest x1 142 us: shards(): lax.psum_scatter(spread.reshape(n_ep * n_tp * rows_b, share), ('ep', 'tp'...]
    all_gather x2, waiting for transfers between devices: 27.4 us -> 88.4 us  [the longest x1 50.3 us: shards(): kv_all = lax.all_gather(sent, ('ep', 'tp'), axis=0, tiled=True)]
    dot_general x31 -> x8, matrix products: 75.3 us -> 19.5 us  [the longest x1 9.17 us: shards(): term = jnp.dot(hidden, w_down[0], preferred_element_type=F32)]
    reduce_sum x11 -> x2, other arithmetic: 23.7 us -> 1.09 us  [the longest x1 0.77 us: shards(): weights_b = jax.nn.softmax(logit_part, axis=-1)]
    pallas_call x0 -> x1, Pallas kernels: none -> 21.7 us  [attention(): pl.pallas_call(functools.partial(attention_kernel, heads), out_shape=jax....]
    all_to_all x1 -> x0, blocking collectives: 18.1 us -> none  [shards(): lax.all_to_all(outgoing, 'ep', split_axis=0, concat_axis=0, tiled=True)]
    all_gather x1 -> x0, blocking collectives: 14.9 us -> none  [shards(): lax.all_gather(rope_key, 'ep', axis=0, tiled=True)]
    all_to_all x1 -> x0, waiting for transfers between devices: 11.1 us -> none  [shards(): lax.all_to_all(finished, 'ep', split_axis=0, concat_axis=0, tiled=True)]
  transfers between devices with their start and end apart: 5 -> 4, of which waited for: 4 -> 4; matrix products, arithmetic and copies ran while one was open for 50% -> 12% of each run, Pallas kernels for 0% -> 7%
where the time goes in v1:
time: 328 us; the launch traced here: 323 us
  waiting for transfers between devices  241 us (73%)
  Pallas kernels  21.7 us (7%)
  matrix products  19.5 us (6%)
  between operations  14.2 us (4%)
  other arithmetic  13.3 us (4%)
  local copies, waits for them, and re-layouts  12.7 us (4%)
    reduce_scatter x1, waiting for transfers between devices, shards(): lax.psum_scatter(spread.reshape(n_ep * n_tp * rows_b, share), ('ep', 'tp'...  142 us
    all_gather x1, waiting for transfers between devices, shards(): kv_all = lax.all_gather(sent, ('ep', 'tp'), axis=0, tiled=True)  50.3 us
    all_gather x1, waiting for transfers between devices, shards(): tok_all = lax.all_gather(sent_b, ('ep', 'tp'), axis=0, tiled=True)  38.1 us
    pallas_call x1, Pallas kernels, attention(): pl.pallas_call(functools.partial(attention_kernel, heads), out_shape=jax....  21.7 us
    reduce_scatter x1, waiting for transfers between devices, shards(): lax.psum_scatter(jnp.dot(attended, w_out, preferred_element_type=F32).ast...  10.8 us
    dot_general x1, matrix products, shards(): term = jnp.dot(hidden, w_down[0], preferred_element_type=F32)  9.17 us
  transfers between devices with their start and end apart: 4, of which 4 were waited for; matrix products, arithmetic and copies ran while one was open for 12% of the time, Pallas kernels for 7%

profile of v1, /device:TPU:1, one launch (start us, length us, event | category | flops | bytes accessed | tf_op | source)
XLA Modules:
  0.0 322.8 jit_solution(11579876051971972246)
XLA Ops:
  7.2 0.0 copy-start
  7.2 0.0 all-gather.3.cloned.1.call-start
  7.3 1.0 fusion.60
  8.3 0.7 convert_element_type.138
  9.0 0.7 constant_dynamic-slice_fusion.2
  9.7 0.1 copy.85
  9.9 1.0 fusion.62
  10.8 0.3 fusion.68
  11.2 0.7 pad_maximum_fusion.1
  11.9 0.0 all-gather.3.cloned.1.call-update
  11.9 0.0 all-gather.5.cloned.1.call-start
  12.0 0.8 fusion.75
  12.7 0.8 fusion.74
  13.5 0.8 subtract_convert_fusion
  14.3 0.1 copy.74
  14.4 0.1 copy.75
  14.5 0.7 convert_element_type.146
  15.2 0.8 fusion.72
  15.9 0.1 copy.73
  16.0 1.0 fusion.55
  17.1 1.0 fusion.57
  18.1 0.8 concatenate.27
  18.9 0.0 all-gather.5.cloned.1.call-update
  18.9 0.0 reduce-scatter.3.cloned.1.call-start
  18.9 0.2 multiply_sine_fusion.1
  19.1 0.1 copy.61
  19.3 0.1 copy.64
  19.5 0.1 pad.53.clone
  19.5 0.1 copy.59
  19.7 0.8 copy.58
  20.5 0.1 copy.68
  20.8 0.2 copy.81
  20.9 0.1 copy.70
  21.1 0.2 copy.82
  21.3 0.1 pad_maximum_fusion.w_ref
  21.4 0.4 copy-done.2
  21.8 0.2 fusion.22
  22.0 0.3 maximum_maximum_fusion.1
  22.4 0.5 fusion.20
  22.9 0.5 fusion.21.q_ref
  23.4 50.3 %all-gather.3.cloned.1.call-done.kv_ref = bf16[4096,288]{1,0:T(8,128)(2,1)} async-done(((bf16[128,288]{1,0:T(8,128)(2,1)}), bf16[4096,288]{1,0:T(8,128)(2,1)}) %all-gather.3.cloned.1.call-update) | async-done | bytes 2359312 | tf_op jit(solution)/shard_map/all_gather | solution.py:150
  73.7 1.9 copy-done.1
  75.6 21.7 %attention.1 = bf16[4,512,64]{2,1,0:T(8,128)(2,1)S(1)} custom-call(bf16[4,512,128]{2,1,0:T(8,128)(2,1)S(1)} %fusion.21.q_ref, bf16[4096,288]{1,0:T(8,128)(2,1)S(1)} %copy-done.1, bf16[288,1024]{1,0:T(8,128)(2,1)S(1)} %pad_maximum_fusion.w_ref), custom_call_target="tpu_custom_call" | custom-call | flops 8589934592 | bytes 8388608 | tf_op jit(solution)/shard_map/attention/pallas_call | solution.py:84
  97.2 0.2 copy.72
  97.5 2.1 convolution_convert_fusion
  99.5 0.0 reduce-scatter.3.cloned.1.call-update
  99.6 0.2 reduce-scatter.5.cloned.1.call-start
  99.8 38.1 %all-gather.5.cloned.1.call-done = bf16[1024,2176]{1,0:T(8,128)(2,1)} async-done(((bf16[32,2176]{1,0:T(8,128)(2,1)}), bf16[1024,2176]{1,0:T(8,128)(2,1)}) %all-gather.5.cloned.1.call-update) | async-done | bytes 4456464 | tf_op jit(solution)/shard_map/all_gather | solution.py:163
  137.9 1.1 slice_convert_fusion
  139.0 0.4 fusion.58
  139.4 0.2 fusion.51
  139.6 0.8 fusion.40
  140.4 0.1 bitcast_select_fusion
  140.5 0.3 select_reduce_fusion
  140.8 1.8 fusion.10
  142.7 1.1 copy-done.11
  143.8 3.0 fusion.6
  146.8 9.2 %multiply_convert_fusion = bf16[384,2048]{1,0:T(8,128)(2,1)} fusion(bf16[1,1024,2048]{2,1,0:T(8,128)(2,1)} %param.33, f32[384]{0:T(512)S(1)} %select_reduce_fusion, f32[384,1024]{1,0:T(8,128)} %fusion.6, bf16[384,2048]{1,0:T(8,128)(2,1)} %copy-done.11, bf16[1,2048,1024]{2,1,0:T(8,128)(2,1)} %param.32), kind=kOutput, calls=%fused_computation.9 | convolution fusion | flops 3225157632 | bytes 13108736 | tf_op jit(solution)/shard_map/dot_general | solution.py:217
  156.0 2.9 reshape.196
  158.9 2.4 convert_bitcast_fusion
  161.3 2.4 copy.77
  163.7 0.0 reduce-scatter.5.cloned.1.call-update
  163.7 10.8 %reduce-scatter.3.cloned.1.call-done = bf16[128,2048]{1,0:T(8,128)(2,1)} async-done(((bf16[512,2048]{1,0:T(8,128)(2,1)}), bf16[128,2048]{1,0:T(8,128)(2,1)}) %reduce-scatter.3.cloned.1.call-update) | async-done | bytes 524304 | tf_op jit(solution)/shard_map/reduce_scatter | solution.py:189
  174.4 141.8 %reduce-scatter.5.cloned.1.call-done = bf16[128,512]{1,0:T(8,128)(2,1)} async-done(((bf16[4096,512]{1,0:T(8,128)(2,1)}), bf16[128,512]{1,0:T(8,128)(2,1)}) %reduce-scatter.5.cloned.1.call-update) | async-done | bytes 131088 | tf_op jit(solution)/shard_map/reduce_scatter | solution.py:226
  (42 shorter events, 0.3 us)
Async XLA Ops:
  7.2 90.3 %copy-start = (bf16[256,2048]{1,0:T(8,128)(2,1)S(1)}, bf16[256,2048]{1,0:T(8,128)(2,1)}, u32[]{:S(2)}) copy-start(bf16[256,2048]{1,0:T(8,128)(2,1)} %param.26) | copy-start | bytes 3145732
  7.2 12.4 %copy-start.5 = (bf16[512,128]{1,0:T(8,128)(2,1)S(1)}, bf16[512,128]{1,0:T(8,128)(2,1)}, u32[]{:S(2)}) copy-start(bf16[512,128]{1,0:T(8,128)(2,1)} %param.23) | copy-start | bytes 393220
  7.2 12.5 %copy-start.9 = (bf16[512]{0:T(512)(128)(2,1)S(1)}, bf16[512]{0:T(512)(128)(2,1)}, u32[]{:S(2)}) copy-start(bf16[512]{0:T(512)(128)(2,1)} %param.20) | copy-start | bytes 3076
  7.2 12.5 %copy-start.3 = (bf16[512,256]{1,0:T(8,128)(2,1)S(1)}, bf16[512,256]{1,0:T(8,128)(2,1)}, u32[]{:S(2)}) copy-start(bf16[512,256]{1,0:T(8,128)(2,1)} %param.22) | copy-start | bytes 786436
  7.2 66.5 %all-gather.3.cloned.1.call-start = ((), (), s32[]{:S(2)}) async-start(), calls=%async_computation.2 | async-start | bytes 3244032 | tf_op jit(solution)/shard_map/all_gather | solution.py:150
  9.8 10.7 %copy-start.6 = (bf16[256,256]{1,0:T(8,128)(2,1)S(1)}, bf16[256,256]{1,0:T(8,128)(2,1)}, u32[]{:S(2)}) copy-start(bf16[256,256]{1,0:T(8,128)(2,1)} %param.24) | copy-start | bytes 393220
  11.9 125.9 %all-gather.5.cloned.1.call-start = ((), (), s32[]{:S(2)}) async-start(), calls=%async_computation.4 | async-start | bytes 4595712 | tf_op jit(solution)/shard_map/all_gather | solution.py:163
  18.9 155.6 %reduce-scatter.3.cloned.1.call-start = ((), (), s32[]{:S(2)}) async-start(), calls=%async_computation.3 | async-start | bytes 2621440 | tf_op jit(solution)/shard_map/reduce_scatter | solution.py:189
  19.1 1.8 copy-start.7
  20.8 1.0 copy-start.2
  21.3 1.1 copy-start.4
  73.7 1.9 copy-start.1
  99.6 216.7 %reduce-scatter.5.cloned.1.call-start = ((), (), s32[]{:S(2)}) async-start(), calls=%async_computation.5 | async-start | bytes 4325376 | tf_op jit(solution)/shard_map/reduce_scatter | solution.py:226
  137.9 3.0 copy-start.8
  140.8 3.0 copy-start.10
  142.7 1.1 copy-start.11
Sparse Core Ops, SparseCore 0:
  12.0 61.5 all-gather.2
  76.5 61.3 all-gather.4
  141.4 32.9 reduce-scatter.2
  177.1 139.0 reduce-scatter.4

commit v2 on v1

--- a/solution.py
+++ b/solution.py
@@ -30,28 +30,169 @@
     return jnp.cos(angles), jnp.sin(angles)
 
 
-def attention_kernel(heads, q_ref, kv_ref, w_ref, out_ref, k_buf, v_buf):
-    keys = kv_ref.shape[0]
+MESH = pl.DeviceIdType.MESH
+
+
+def remote(src, dst, send, recv, ep, tp):
+    return pltpu.make_async_remote_copy(
+        src_ref=src,
+        dst_ref=dst,
+        send_sem=send,
+        recv_sem=recv,
+        device_id={"ep": ep, "tp": tp},
+        device_id_type=MESH,
+    )
+
+
+def loop(count, body, start=0):
+    def step(i, c):
+        body(i)
+        return c
+
+    lax.fori_loop(start, count, step, 0)
+
+
+class Gather:
+    def __init__(self, n_ep, n_tp, own, buf, local, recv, send_z, send_t, send_c):
+        self.n_tp, self.nz = n_tp, n_ep // 2
+        self.own, self.buf, self.local = own, buf, local
+        self.recv, self.send_z, self.send_t, self.send_c = recv, send_z, send_t, send_c
+        ep = lax.axis_index("ep")
+        self.z, self.core, self.t = ep // 2, ep % 2, lax.axis_index("tp")
+        self.ep = ep
+
+    def slot(self, z, core, t):
+        return (z * 2 + core) * self.n_tp + t
+
+    def at_z(self, d):
+        return (self.z + self.nz - d) % self.nz
+
+    def at_t(self, d):
+        return (self.t + self.n_tp - d) % self.n_tp
+
+    def copy_z(self, d):
+        me = self.slot(self.z, self.core, self.t)
+        to = (self.z + d) % self.nz
+        return remote(
+            self.own, self.buf.at[me], self.send_z.at[d], self.recv.at[me], to * 2 + self.core, self.t
+        )
+
+    def copy_t(self, dz, d):
+        s = self.slot(self.at_z(dz), self.core, self.t)
+        to = (self.t + d) % self.n_tp
+        return remote(
+            self.buf.at[s], self.buf.at[s], self.send_t.at[dz * self.n_tp + d], self.recv.at[s], self.ep, to
+        )
+
+    def copy_c(self, dz, d):
+        s = self.slot(self.at_z(dz), self.core, self.at_t(d))
+        return remote(
+            self.buf.at[s],
+            self.buf.at[s],
+            self.send_c.at[dz * self.n_tp + d],
+            self.recv.at[s],
+            self.z * 2 + 1 - self.core,
+            self.t,
+        )
+
+    def landed(self, s):
+        remote(self.own, self.buf.at[s], self.local, self.recv.at[s], self.ep, self.t).wait_recv()
+
+    def start(self):
+        loop(self.nz, lambda d: self.copy_z(d).start(), 1)
+        me = self.slot(self.z, self.core, self.t)
+        mine = pltpu.make_async_copy(self.own, self.buf.at[me], self.local)
+        mine.start()
+        mine.wait()
+
+    def over_tp(self):
+        def one(dz):
+            @pl.when(dz > 0)
+            def _():
+                self.landed(self.slot(self.at_z(dz), self.core, self.t))
+
+            loop(self.n_tp, lambda d: self.copy_t(dz, d).start(), 1)
+            self.copy_c(dz, 0).start()
+
+        loop(self.nz, one)
+
+    def to_sibling(self):
+        def one(dz):
+            def inner(d):
+                self.landed(self.slot(self.at_z(dz), self.core, self.at_t(d)))
+                self.copy_c(dz, d).start()
+
+            loop(self.n_tp, inner, 1)
+
+        loop(self.nz, one)
+
+    def finish(self):
+        def one(dz):
+            def inner(d):
+                self.landed(self.slot(self.at_z(dz), 1 - self.core, self.at_t(d)))
+                self.copy_c(dz, d).wait_send()
+
+            loop(self.n_tp, inner)
+            loop(self.n_tp, lambda d: self.copy_t(dz, d).wait_send(), 1)
+
+        loop(self.nz, one)
+        loop(self.nz, lambda d: self.copy_z(d).wait_send(), 1)
+
+
+def greet(n_ep, n_tp, every_ep):
+    ep, t = lax.axis_index("ep"), lax.axis_index("tp")
+    barrier = pltpu.get_barrier_semaphore()
+
+    def hello(e, tp):
+        pl.semaphore_signal(barrier, inc=1, device_id={"ep": e, "tp": tp}, device_id_type=MESH)
+
+    loop(n_tp, lambda d: hello(ep, (t + d) % n_tp), 1)
+    if every_ep:
+        loop(n_ep, lambda d: hello((ep + d) % n_ep, t), 1)
+        pl.semaphore_wait(barrier, n_tp + n_ep - 2)
+    else:
+        nz = n_ep // 2
+        loop(nz, lambda d: hello((ep // 2 + d) % nz * 2 + ep % 2, t), 1)
+        hello(ep // 2 * 2 + 1 - ep % 2, t)
+        pl.semaphore_wait(barrier, n_tp + nz - 1)
+
+
+def attention_kernel(
+    heads, n_ep, n_tp, sent_ref, tok_ref, q_ref, w_ref, out_ref, tok_out, kv_buf, k_buf, v_buf, *sems
+):
+    part, lat = sent_ref.shape[0], w_ref.shape[0]
+    keys = n_ep * n_tp * part
     rows = q_ref.shape[1]
     scale = (NOPE + ROPE) ** (-0.5) * math.log2(math.e)
-    chunk = 512
     q_block = min(256, rows)
     k_block = 1024
     wide = heads * LANES
-
-    def project(c, _):
+    latents = Gather(n_ep, n_tp, sent_ref, kv_buf, *sems[:5])
+    tokens = Gather(n_ep, n_tp, tok_ref, tok_out, *sems[5:])
+    greet(n_ep, n_tp, False)
+    latents.start()
+    latents.over_tp()
+    tokens.start()
+    latents.to_sibling()
+    latents.finish()
+    tokens.over_tp()
+    group = max(1, 512 // part)
+    chunk = group * part
+
+    def project(c):
         here = pl.ds(pl.multiple_of(c * chunk, chunk), chunk)
-        up = jnp.dot(kv_ref[here, :], w_ref[...], preferred_element_type=F32)
+        block = kv_buf[pl.ds(c * group, group)].reshape(chunk, kv_buf.shape[2])
+        up = jnp.dot(block[:, :lat], w_ref[...], preferred_element_type=F32)
+        turned = block[:, lat:].astype(F32)
         lane = lax.broadcasted_iota(jnp.int32, (chunk, LANES), 1)
         for h in range(heads):
-            k_buf[h, here, :] = up[:, h * LANES : (h + 1) * LANES].astype(BF)
+            k_buf[h, here, :] = (up[:, h * LANES : (h + 1) * LANES] + turned).astype(BF)
             v = up[:, wide + h * LANES : wide + (h + 1) * LANES]
             v_buf[h, here, :] = jnp.where(lane < VDIM, v, 1.0).astype(BF)
-        return 0
-
-    lax.fori_loop(0, keys // chunk, project, 0)
-
-    def attend(step, _):
+
+    loop(keys // chunk, project)
+
+    def attend(step):
         h = step // (rows // q_block)
         b = step % (rows // q_block)
         here = pl.ds(pl.multiple_of(b * q_block, q_block), q_block)
@@ -72,30 +213,217 @@
                 acc = acc * jnp.exp2((top - new_top) * scale) + pv
             top = new_top
         out_ref[h, here, :] = (acc[:, :VDIM] / acc[:, VDIM : VDIM + 1]).astype(BF)
-        return 0
-
-    lax.fori_loop(0, heads * (rows // q_block), attend, 0)
-
-
-def attention(q, kv, w):
+
+    loop(heads * (rows // q_block), attend)
+    tokens.to_sibling()
+    tokens.finish()
+
+
+def gather_sems(n_ep, n_tp):
+    dma = pltpu.SemaphoreType.DMA
+    blocks = n_ep // 2 * n_tp
+    return [dma, dma((n_ep * n_tp,)), dma((n_ep // 2,)), dma((blocks,)), dma((blocks,))]
+
+
+def attention(n_ep, n_tp, sent, tok, q, w):
     heads, rows, _ = q.shape
-    keys = kv.shape[0]
+    part = sent.shape[0]
+    n = n_ep * n_tp
+    keys = part * n
     flops = 4 * heads * rows * keys * 256
+    vmem = pl.BlockSpec(memory_space=pltpu.VMEM)
     return pl.pallas_call(
-        functools.partial(attention_kernel, heads),
-        out_shape=jax.ShapeDtypeStruct((heads, rows, VDIM), BF),
-        in_specs=[pl.BlockSpec(memory_space=pltpu.VMEM)] * 3,
-        out_specs=pl.BlockSpec(memory_space=pltpu.VMEM),
+        functools.partial(attention_kernel, heads, n_ep, n_tp),
+        out_shape=(
+            jax.ShapeDtypeStruct((heads, rows, VDIM), BF),
+            jax.ShapeDtypeStruct((n,) + tok.shape, BF),
+        ),
+        in_specs=[vmem] * 4,
+        out_specs=(vmem, vmem),
         scratch_shapes=[
+            pltpu.VMEM((n,) + sent.shape, BF),
             pltpu.VMEM((heads, keys, LANES), BF),
             pltpu.VMEM((heads, keys, LANES), BF),
-        ],
-        compiler_params=pltpu.CompilerParams(vmem_limit_bytes=48 * 1024 * 1024),
+        ]
+        + gather_sems(n_ep, n_tp)
+        + gather_sems(n_ep, n_tp),
+        compiler_params=pltpu.CompilerParams(
+            vmem_limit_bytes=60 * 1024 * 1024, collective_id=0, has_side_effects=True
+        ),
         cost_estimate=pl.CostEstimate(
             flops=flops, bytes_accessed=8 * 1024 * 1024, transcendentals=heads * rows * keys
         ),
         name="attention",
-    )(q, kv, w)
+    )(sent, tok, q, w)
+
+
+def experts_kernel(
+    n_ep,
+    n_tp,
+    att_ref,
+    wo_ref,
+    piece_ref,
+    scale_ref,
+    own_ref,
+    wg_hbm,
+    wu_hbm,
+    wd_hbm,
+    mix_ref,
+    exp_ref,
+    wg,
+    wu,
+    wd,
+    hid,
+    p_send,
+    p_recv,
+    t_send,
+    t_recv,
+    e_send,
+    e_recv,
+    w_sem,
+    ps,
+    pr,
+    ts,
+    tr,
+    es,
+    er,
+):
+    ep, t = lax.axis_index("ep"), lax.axis_index("tp")
+    part = mix_ref.shape[0]
+    total, share = t_send.shape[1:]
+    room = e_send.shape[1]
+    loads = [
+        pltpu.make_async_copy(a, b, w_sem.at[i])
+        for i, (a, b) in enumerate(((wg_hbm, wg), (wu_hbm, wu), (wd_hbm, wd)))
+    ]
+    for load in loads:
+        load.start()
+    greet(n_ep, n_tp, True)
+
+    def to_tp(send, recv, ss, rs, d):
+        to = (t + d) % n_tp
+        return remote(send.at[to], recv.at[t], ss.at[d], rs.at[t], ep, to)
+
+    def from_tp(send, recv, ss, rs, d):
+        frm = (t + n_tp - d) % n_tp
+        remote(send.at[frm], recv.at[frm], ss.at[0], rs.at[frm], ep, frm).wait_recv()
+        return frm
+
+    mixer = (p_send, p_recv, ps, pr)
+    terms = (t_send, t_recv, ts, tr)
+
+    def project(d):
+        to = (t + d) % n_tp
+        rows = att_ref[pl.ds(pl.multiple_of(to * part, part), part), :]
+        p_send[to] = jnp.dot(rows, wo_ref[...], preferred_element_type=F32).astype(BF)
+
+        @pl.when(d < n_tp)
+        def _():
+            to_tp(*mixer, d).start()
+
+    loop(n_tp + 1, project, 1)
+
+    step = 256
+    loads[0].wait()
+    loads[1].wait()
+
+    def up(c):
+        at = pl.ds(pl.multiple_of(c * step, step), step)
+        g = jnp.dot(piece_ref[...], wg[:, at], preferred_element_type=F32)
+        u = jnp.dot(piece_ref[...], wu[:, at], preferred_element_type=F32)
+        hid[:, at] = (g / (1.0 + jnp.exp(-g)) * u).astype(BF)
+
+    loop(hid.shape[1] // step, up)
+    loads[2].wait()
+
+    def down(d):
+        to = (t + d) % n_tp
+        at = pl.ds(pl.multiple_of(to * share, share), share)
+        t_send[to] = jnp.dot(hid[...], wd[:, at], preferred_element_type=F32).astype(BF)
+
+        @pl.when(d < n_tp)
+        def _():
+            to_tp(*terms, d).start()
+
+    loop(n_tp + 1, down, 1)
+
+    def reduced(send, group):
+        acc = send[t].astype(F32)
+        for d in range(1, n_tp):
+            frm = from_tp(*group, d)
+            acc = acc + group[1][frm].astype(F32)
+        return acc
+
+    mix_ref[...] = reduced(p_send, mixer).astype(BF)
+    out = (reduced(t_send, terms) * scale_ref[:, :1]).astype(BF)
+    e_send[...] = out.reshape(n_ep, room, share)
+    e_recv[ep] = e_send[ep]
+
+    def to_ep(d):
+        to = (ep + d) % n_ep
+        return remote(e_send.at[to], e_recv.at[ep], es.at[d], er.at[ep], to, t)
+
+    loop(n_ep, lambda d: to_ep(d).start(), 1)
+
+    def arrived(d):
+        frm = (ep + n_ep - d) % n_ep
+        remote(e_send.at[frm], e_recv.at[frm], es.at[0], er.at[frm], frm, t).wait_recv()
+
+    loop(n_ep, arrived, 1)
+    back = e_recv[...].reshape(n_ep * room, share)
+    exp_ref[...] = jnp.dot(own_ref[...], back, preferred_element_type=F32).astype(BF)
+
+    def drain(d):
+        to_tp(*mixer, d).wait_send()
+        to_tp(*terms, d).wait_send()
+
+    loop(n_tp, drain, 1)
+    loop(n_ep, lambda d: to_ep(d).wait_send(), 1)
+
+
+def experts(n_ep, n_tp, room, att, w_out, piece, scale, own, w_gate, w_up, w_down):
+    vmem = pl.BlockSpec(memory_space=pltpu.VMEM)
+    hbm = pl.BlockSpec(memory_space=pl.ANY)
+    dma = pltpu.SemaphoreType.DMA
+    width = w_out.shape[1]
+    total = piece.shape[0]
+    part, share = att.shape[0] // n_tp, width // n_tp
+    flops = 6 * total * width * w_gate.shape[1] + 2 * att.shape[0] * att.shape[1] * width
+    return pl.pallas_call(
+        functools.partial(experts_kernel, n_ep, n_tp),
+        out_shape=(
+            jax.ShapeDtypeStruct((part, width), BF),
+            jax.ShapeDtypeStruct((own.shape[0], share), BF),
+        ),
+        in_specs=[vmem] * 5 + [hbm] * 3,
+        out_specs=(vmem, vmem),
+        scratch_shapes=[
+            pltpu.VMEM(w_gate.shape, BF),
+            pltpu.VMEM(w_up.shape, BF),
+            pltpu.VMEM(w_down.shape, BF),
+            pltpu.VMEM((total, w_gate.shape[1]), BF),
+            pltpu.VMEM((n_tp, part, width), BF),
+            pltpu.VMEM((n_tp, part, width), BF),
+            pltpu.VMEM((n_tp, total, share), BF),
+            pltpu.VMEM((n_tp, total, share), BF),
+            pltpu.VMEM((n_ep, room, share), BF),
+            pltpu.VMEM((n_ep, room, share), BF),
+            dma((3,)),
+            dma((n_tp,)),
+            dma((n_tp,)),
+            dma((n_tp,)),
+            dma((n_tp,)),
+            dma((n_ep,)),
+            dma((n_ep,)),
+        ],
+        compiler_params=pltpu.CompilerParams(
+            vmem_limit_bytes=60 * 1024 * 1024, collective_id=1, has_side_effects=True
+        ),
+        cost_estimate=pl.CostEstimate(
+            flops=flops, bytes_accessed=20 * 1024 * 1024, transcendentals=0
+        ),
+        name="experts",
+    )(att, w_out, piece, scale, own, w_gate, w_up, w_down)
 
 
 def lay_heads(weights, heads, width, offset):
@@ -142,12 +470,13 @@
     sent = jnp.concatenate(
         [
             rms_rows(kv_part, kv_gain),
+            jnp.zeros((part, NOPE), BF),
             (first * cosine - second * sine).astype(BF),
             (first * sine + second * cosine).astype(BF),
+            jnp.zeros((part, LANES - NOPE - ROPE), BF),
         ],
         axis=1,
     )
-    kv_all = lax.all_gather(sent, ("ep", "tp"), axis=0, tiled=True)
 
     part_b = rows_b // n_tp
     tok_part = lax.dynamic_slice_in_dim(tokens_b, t_at * part_b, part_b, 0)
@@ -160,7 +489,6 @@
         [route_part.astype(BF), high, low, jnp.zeros((part_b, LANES - 6), BF)], axis=1
     )
     sent_b = jnp.concatenate([rms_rows(tok_part, norm_gain_b), extra], axis=1)
-    tok_all = lax.all_gather(sent_b, ("ep", "tp"), axis=0, tiled=True)
 
     q_normed = rms_rows(q_latent, q_gain)
     w_nope = lay_heads(w_q_nope, heads, NOPE, 0)
@@ -177,23 +505,14 @@
     swapped = jnp.einsum("rd,dhl->hrl", q_normed, w_turned, preferred_element_type=F32)
     q = (plain * cos_row + swapped * sin_row).astype(BF)
 
-    place = jnp.pad(jnp.eye(ROPE, dtype=BF), ((0, 0), (NOPE, LANES - NOPE - ROPE)))
-    place = jnp.broadcast_to(place[:, None, :], (ROPE, heads, LANES))
-    w_keys = jnp.concatenate([lay_heads(w_k_nope, heads, NOPE, 0), place], axis=0)
-    w_vals = jnp.pad(lay_heads(w_value, heads, VDIM, 0), ((0, ROPE), (0, 0), (0, 0)))
-    w_kv = jnp.concatenate(
-        [w_keys.reshape(-1, heads * LANES), w_vals.reshape(-1, heads * LANES)], axis=1
-    )
-    attended = attention(q, kv_all, w_kv)
+    w_keys = lay_heads(w_k_nope, heads, NOPE, 0).reshape(-1, heads * LANES)
+    w_vals = lay_heads(w_value, heads, VDIM, 0).reshape(-1, heads * LANES)
+    w_kv = jnp.concatenate([w_keys, w_vals], axis=1)
+    attended, tok_all = attention(n_ep, n_tp, sent, sent_b, q, w_kv)
     attended = attended.transpose(1, 0, 2).reshape(own_rows, heads * VDIM)
-    mixer_out = lax.psum_scatter(
-        jnp.dot(attended, w_out, preferred_element_type=F32).astype(BF),
-        "tp",
-        scatter_dimension=0,
-        tiled=True,
-    )
-
-    room = 3 * rows_b // n_ep
+    tok_all = tok_all.reshape(n_ep * rows_b, width + LANES)
+
+    room = -(-(3 * rows_b // n_ep) // 16) * 16
     total_b = tok_all.shape[0]
     info = tok_all[:, width : width + LANES].astype(F32)
     me = e_at.astype(F32)
@@ -211,20 +530,14 @@
     pick = chosen.astype(BF)
     row_weight = jnp.sum(jnp.where(chosen, weight[None, :], 0.0), axis=1, keepdims=True)
     piece = jnp.dot(pick, tok_all[:, :width], preferred_element_type=F32).astype(BF)
-    gate = jnp.dot(piece, w_gate[0], preferred_element_type=F32)
-    up = jnp.dot(piece, w_up[0], preferred_element_type=F32)
-    hidden = (jax.nn.silu(gate) * up).astype(BF)
-    term = jnp.dot(hidden, w_down[0], preferred_element_type=F32)
-    scaled = (term * row_weight).astype(BF)
-    share = width // n_tp
-    spread = jnp.einsum(
-        "reb,rjc->ejbc",
-        pick.reshape(n_ep * room, n_ep, rows_b),
-        scaled.reshape(n_ep * room, n_tp, share),
-        preferred_element_type=F32,
-    ).astype(BF)
-    expert_mix = lax.psum_scatter(
-        spread.reshape(n_ep * n_tp * rows_b, share), ("ep", "tp"), scatter_dimension=0, tiled=True
+    named = (routes[:, :, None] == jnp.arange(n_ep, dtype=jnp.int32)).astype(F32)
+    used = jnp.sum(named, axis=1)
+    ahead = jnp.dot(before.T, used.astype(BF), preferred_element_type=F32)
+    own = (ahead[:, :, None] == jnp.arange(room, dtype=F32)) & (used[:, :, None] > 0)
+    own = own.astype(BF).reshape(rows_b, n_ep * room)
+    scale = jnp.broadcast_to(row_weight, (n_ep * room, LANES))
+    mixer_out, expert_mix = experts(
+        n_ep, n_tp, room, attended, w_out, piece, scale, own, w_gate[0], w_up[0], w_down[0]
     )
     return (mixer_out, expert_mix)
 

time: 328 us -> 147 us (0.45); the launches traced: 323 us -> 147 us
  waiting for transfers between devices: 241 us -> 0 us
  Pallas kernels: 21.7 us -> 113 us
  between operations: 14.2 us -> 0.99 us
  matrix products: 19.5 us -> 7.23 us
    reduce_scatter x2 -> x0, waiting for transfers between devices: 153 us -> none  [the longest x1 142 us: shards(): lax.psum_scatter(spread.reshape(n_ep * n_tp * rows_b, share), ('ep', 'tp'...]
    pallas_call x1 -> x2, Pallas kernels: 21.7 us -> 113 us  [the longest x1 57.4 us: attention(): pl.pallas_call(functools.partial(attention_kernel, heads, n_ep, n_tp), ou...]
    all_gather x2 -> x0, waiting for transfers between devices: 88.4 us -> none  [the longest x1 50.3 us: shards(): kv_all = lax.all_gather(sent, ('ep', 'tp'), axis=0, tiled=True)]
    dot_general x4 -> x1, matrix products: 16.6 us -> 0.13 us  [shards(): ahead = jnp.dot(before.T, used.astype(BF), preferred_element_type=F32)]
    dot_general x1, matrix products: 1.83 us -> 5.23 us  [shards(): jnp.dot(pick, tok_all[:, :width], preferred_element_type=F32).astype(BF)]
  transfers between devices with their start and end apart: 4 -> 0, of which waited for: 4 -> 0; matrix products, arithmetic and copies ran while one was open for 12% -> 0% of each run, Pallas kernels for 7% -> 0%
where the time goes in v2:
time: 147 us
  Pallas kernels  113 us (77%)
  local copies, waits for them, and re-layouts  13.4 us (9%)
  other arithmetic  11.8 us (8%)
  matrix products  7.23 us (5%)
    pallas_call x1, Pallas kernels, attention(): pl.pallas_call(functools.partial(attention_kernel, heads, n_ep, n_tp), ou...  57.4 us
    pallas_call x1, Pallas kernels, experts(): pl.pallas_call(functools.partial(experts_kernel, n_ep, n_tp), out_shape=(...  55.9 us
    unnamed x18, local copies, waits for them, and re-layouts  6.2 us
    dot_general x1, matrix products, shards(): jnp.dot(pick, tok_all[:, :width], preferred_element_type=F32).astype(BF)  5.23 us
    convert_element_type x5, other arithmetic, rms_rows(): return (scaled * gain.astype(F32)).astype(BF)  3.96 us
    reduce_sum x3, other arithmetic, rms_rows(): jnp.mean(wide * wide, axis=-1, keepdims=True) + EPSILON  3.24 us

profile of v2, /device:TPU:1, one launch (start us, length us, event | category | flops | bytes accessed | tf_op | source)
XLA Modules:
  0.0 146.8 jit_solution(2313774995381595719)
XLA Ops:
  0.6 0.0 copy-start
  0.6 0.0 copy-start.3
  0.7 1.0 fusion.35
  1.7 1.0 fusion.31
  2.8 0.1 pad.34.clone
  2.9 0.7 convert_element_type.121
  3.5 0.7 constant_dynamic-slice_fusion.1
  4.3 0.8 fusion.60
  5.0 0.7 convert_element_type.135
  5.7 1.2 fusion.11
  7.0 0.7 convert_reduce_fusion
  7.7 0.1 fusion.46
  7.8 0.1 eq.88
  7.9 0.0 copy-done
  7.9 0.7 convert_element_type.128
  8.6 0.1 copy.90
  8.7 0.2 fusion.48
  8.9 0.1 subtract_convert_fusion
  9.0 0.1 copy.89
  9.1 0.1 copy.88
  9.2 0.3 fusion.45
  9.6 0.2 copy.82
  9.7 0.2 multiply_sine_fusion.1
  9.9 0.9 fusion.37
  10.9 0.8 concatenate.18.sent_ref
  11.6 1.0 fusion.33
  12.7 0.8 concatenate.19.tok_ref
  13.4 1.0 copy.68
  14.4 0.0 copy-start.2
  14.5 1.0 copy.75
  15.5 0.0 copy-start.1
  15.5 0.1 copy.86
  15.7 0.0 copy-done.3
  15.7 0.1 copy.77
  15.8 0.1 copy.87
  16.0 0.9 pad_maximum_fusion.w_ref
  16.9 0.1 copy.81
  17.0 0.7 and_convert_fusion.own_ref
  17.7 0.1 copy.73
  17.8 0.1 copy.70
  18.0 0.3 maximum_maximum_fusion.1
  18.3 0.0 copy-done.2
  18.3 0.1 copy.67
  18.5 0.0 copy-done.1
  18.5 0.5 fusion.7
  19.0 1.3 fusion.8.q_ref
  20.3 57.4 %attention.1 = (bf16[4,512,64]{2,1,0:T(8,128)(2,1)}, bf16[32,32,2176]{2,1,0:T(8,128)(2,1)}) custom-call(bf16[128,384]{1,0:T(8,128)(2,1)} %concatenate.18.sent_ref, bf16[32,2176]{1,0:T(8,128)(2,1)} %concatenate.19.tok_ref, bf16[4,512,128]{2,1,0:T(8,128)(2,1)} %fusion.8.q_ref, bf16[256,1024]{1,0:T(8,128)(2,1)} %pad_maximum_fusion.w_ref), custom_call_target="tpu_custom_call" | custom-call | flops 8589934592 | bytes 8388608 | tf_op jit(solution)/shard_map/attention/pallas_call | solution.py:235
  77.6 1.2 copy.79
  78.9 0.8 copy.83.att_ref
  79.7 1.0 slice.52
  80.7 0.1 copy.91
  81.0 0.1 fusion.10
  81.1 5.2 %fusion.2.piece_ref = bf16[384,2048]{1,0:T(8,128)(2,1)} fusion(bf16[1024,2176]{1,0:T(8,128)(2,1)} %bitcast.51, f32[1024]{0:T(1024)S(1)} %fusion.10), kind=kOutput, calls=%fused_computation.2 | convolution fusion | flops 1611792384 | bytes 5771264 | tf_op jit(solution)/shard_map/dot_general | solution.py:532
  86.3 0.3 select_reduce_fusion
  86.6 0.8 broadcast_in_dim.36.scale_ref
  87.4 55.9 %experts.1 = (bf16[128,2048]{1,0:T(8,128)(2,1)}, bf16[128,512]{1,0:T(8,128)(2,1)}) custom-call(bf16[512,256]{1,0:T(8,128)(2,1)} %copy.83.att_ref, bf16[256,2048]{1,0:T(8,128)(2,1)} %wo_ref.1, bf16[384,2048]{1,0:T(8,128)(2,1)} %fusion.2.piece_ref, f32[384,128]{1,0:T(8,128)} %broadcast_in_dim.36.scale_ref, bf16[128,384]{1,0:T(8,128)(2,1)} %and_convert_fusion.own_ref, ...), custom_call_target="tpu_custom_call" | custom-call | flops 5368709120 | bytes 20971520 | tf_op jit(solution)/shard_map/experts/pallas_call | solution.py:392
  143.3 1.9 %copy.95 = bf16[128,2048]{1,0:T(8,128)(2,1)} copy(bf16[128,2048]{1,0:T(8,128)(2,1)} %get-tuple-element.22) | data formatting | bytes 1048576
  145.2 1.6 %copy.96 = bf16[128,512]{1,0:T(8,128)(2,1)} copy(bf16[128,512]{1,0:T(8,128)(2,1)} %get-tuple-element.23) | data formatting | bytes 262144
  (29 shorter events, 0.3 us)
Async XLA Ops:
  0.6 7.3 %copy-start = (bf16[512,32]{0,1:T(8,128)(2,1)S(1)}, bf16[512,32]{0,1:T(8,128)(2,1)}, u32[]{:S(2)}) copy-start(bf16[512,32]{0,1:T(8,128)(2,1)} %param.19) | copy-start | bytes 98308
  0.6 15.1 %copy-start.3 = (bf16[256,256]{1,0:T(8,128)(2,1)S(1)}, bf16[256,256]{1,0:T(8,128)(2,1)}, u32[]{:S(2)}) copy-start(bf16[256,256]{1,0:T(8,128)(2,1)} %param.25) | copy-start | bytes 393220
  14.4 3.9 %copy-start.2 = (bf16[512,256]{1,0:T(8,128)(2,1)S(1)}, bf16[512,256]{1,0:T(8,128)(2,1)}, u32[]{:S(2)}) copy-start(bf16[512,256]{1,0:T(8,128)(2,1)} %param.22) | copy-start | bytes 786436
  15.5 2.9 %copy-start.1 = (bf16[512,512]{1,0:T(8,128)(2,1)S(1)}, bf16[512,512]{1,0:T(8,128)(2,1)}, u32[]{:S(2)}) copy-start(bf16[512,512]{1,0:T(8,128)(2,1)} %param.17) | copy-start | bytes 1572868

commit v3 on v2

--- a/solution.py
+++ b/solution.py
@@ -158,11 +158,31 @@
 
 
 def attention_kernel(
-    heads, n_ep, n_tp, sent_ref, tok_ref, q_ref, w_ref, out_ref, tok_out, kv_buf, k_buf, v_buf, *sems
+    heads,
+    n_ep,
+    n_tp,
+    sent_ref,
+    tok_ref,
+    lat_ref,
+    gain_ref,
+    cos_ref,
+    sin_ref,
+    qn_ref,
+    qr_ref,
+    wk_ref,
+    wv_ref,
+    out_ref,
+    tok_out,
+    kv_buf,
+    k_buf,
+    v_buf,
+    q_ref,
+    w_ref,
+    *sems,
 ):
-    part, lat = sent_ref.shape[0], w_ref.shape[0]
+    part, lat = sent_ref.shape[0], wk_ref.shape[0]
     keys = n_ep * n_tp * part
-    rows = q_ref.shape[1]
+    rows = lat_ref.shape[0]
     scale = (NOPE + ROPE) ** (-0.5) * math.log2(math.e)
     q_block = min(256, rows)
     k_block = 1024
@@ -173,6 +193,25 @@
     latents.start()
     latents.over_tp()
     tokens.start()
+
+    def beside(parts, depth, width):
+        filler = jnp.zeros((depth, LANES - width), BF)
+        return jnp.concatenate(parts + [filler], axis=1)
+
+    for h in range(heads):
+        nope, value = slice(h * NOPE, (h + 1) * NOPE), slice(h * VDIM, (h + 1) * VDIM)
+        w_ref[:, h * LANES : (h + 1) * LANES] = beside([wk_ref[:, nope]], lat, NOPE)
+        w_ref[:, wide + h * LANES : wide + (h + 1) * LANES] = beside([wv_ref[:, value]], lat, VDIM)
+    normed = rms_rows(lat_ref[...], gain_ref[...])
+    deep, half = lat_ref.shape[1], ROPE // 2
+    for h in range(heads):
+        turn = qr_ref[:, h * ROPE : (h + 1) * ROPE]
+        plain = beside([qn_ref[:, h * NOPE : (h + 1) * NOPE], turn], deep, NOPE + ROPE)
+        blank = jnp.zeros((deep, NOPE), BF)
+        turned = beside([blank, -turn[:, half:], turn[:, :half]], deep, NOPE + ROPE)
+        q = jnp.dot(normed, plain, preferred_element_type=F32) * cos_ref[...]
+        q = q + jnp.dot(normed, turned, preferred_element_type=F32) * sin_ref[...]
+        q_ref[h] = q.astype(BF)
     latents.to_sibling()
     latents.finish()
     tokens.over_tp()
@@ -192,29 +231,29 @@
 
     loop(keys // chunk, project)
 
-    def attend(step):
-        h = step // (rows // q_block)
-        b = step % (rows // q_block)
-        here = pl.ds(pl.multiple_of(b * q_block, q_block), q_block)
+    def attend_head(h, here):
         q = q_ref[h, here, :]
-        top = jnp.full((q_block, 1), -jnp.inf, F32)
-        acc = jnp.zeros((q_block, LANES), F32)
+        top, acc = None, None
         for j in range(keys // k_block):
             at = slice(j * k_block, (j + 1) * k_block)
             s = lax.dot_general(
                 q, k_buf[h, at, :], (((1,), (1,)), ((), ())), preferred_element_type=F32
             )
-            new_top = jnp.maximum(top, jnp.max(s, axis=-1, keepdims=True))
+            new_top = jnp.max(s, axis=-1, keepdims=True)
+            if j > 0:
+                new_top = jnp.maximum(top, new_top)
             p = jnp.exp2((s - new_top) * scale).astype(BF)
             pv = jnp.dot(p, v_buf[h, at, :], preferred_element_type=F32)
-            if j == 0:
-                acc = pv
-            else:
-                acc = acc * jnp.exp2((top - new_top) * scale) + pv
+            acc = pv if j == 0 else acc * jnp.exp2((top - new_top) * scale) + pv
             top = new_top
-        out_ref[h, here, :] = (acc[:, :VDIM] / acc[:, VDIM : VDIM + 1]).astype(BF)
-
-    loop(heads * (rows // q_block), attend)
+        return (acc[:, :VDIM] / acc[:, VDIM : VDIM + 1]).astype(BF)
+
+    def attend(step):
+        here = pl.ds(pl.multiple_of(step * q_block, q_block), q_block)
+        done = [attend_head(h, here) for h in range(heads)]
+        out_ref[here, :] = done[0] if heads == 1 else jnp.concatenate(done, axis=1)
+
+    loop(rows // q_block, attend)
     tokens.to_sibling()
     tokens.finish()
 
@@ -225,8 +264,9 @@
     return [dma, dma((n_ep * n_tp,)), dma((n_ep // 2,)), dma((blocks,)), dma((blocks,))]
 
 
-def attention(n_ep, n_tp, sent, tok, q, w):
-    heads, rows, _ = q.shape
+def attention(n_ep, n_tp, heads, *operands):
+    sent, tok, latent = operands[:3]
+    rows = latent.shape[0]
     part = sent.shape[0]
     n = n_ep * n_tp
     keys = part * n
@@ -235,15 +275,17 @@
     return pl.pallas_call(
         functools.partial(attention_kernel, heads, n_ep, n_tp),
         out_shape=(
-            jax.ShapeDtypeStruct((heads, rows, VDIM), BF),
+            jax.ShapeDtypeStruct((rows, heads * VDIM), BF),
             jax.ShapeDtypeStruct((n,) + tok.shape, BF),
         ),
-        in_specs=[vmem] * 4,
+        in_specs=[vmem] * len(operands),
         out_specs=(vmem, vmem),
         scratch_shapes=[
             pltpu.VMEM((n,) + sent.shape, BF),
             pltpu.VMEM((heads, keys, LANES), BF),
             pltpu.VMEM((heads, keys, LANES), BF),
+            pltpu.VMEM((heads, rows, LANES), BF),
+            pltpu.VMEM((operands[-1].shape[0], 2 * heads * LANES), BF),
         ]
         + gather_sems(n_ep, n_tp)
         + gather_sems(n_ep, n_tp),
@@ -254,7 +296,7 @@
             flops=flops, bytes_accessed=8 * 1024 * 1024, transcendentals=heads * rows * keys
         ),
         name="attention",
-    )(sent, tok, q, w)
+    )(*operands)
 
 
 def experts_kernel(
@@ -262,17 +304,20 @@
     n_tp,
     att_ref,
     wo_ref,
-    piece_ref,
+    pick_ref,
     scale_ref,
     own_ref,
     wg_hbm,
     wu_hbm,
     wd_hbm,
+    tok_hbm,
     mix_ref,
     exp_ref,
     wg,
     wu,
     wd,
+    tok,
+    piece_ref,
     hid,
     p_send,
     p_recv,
@@ -294,7 +339,9 @@
     room = e_send.shape[1]
     loads = [
         pltpu.make_async_copy(a, b, w_sem.at[i])
-        for i, (a, b) in enumerate(((wg_hbm, wg), (wu_hbm, wu), (wd_hbm, wd)))
+        for i, (a, b) in enumerate(
+            ((tok_hbm, tok), (wg_hbm, wg), (wu_hbm, wu), (wd_hbm, wd))
+        )
     ]
     for load in loads:
         load.start()
@@ -323,9 +370,18 @@
 
     loop(n_tp + 1, project, 1)
 
+    loads[0].wait()
+    span = 512
+
+    def select(c):
+        at = pl.ds(pl.multiple_of(c * span, span), span)
+        rows = jnp.dot(pick_ref[...], tok[:, at], preferred_element_type=F32)
+        piece_ref[:, at] = rows.astype(BF)
+
+    loop(piece_ref.shape[1] // span, select)
     step = 256
-    loads[0].wait()
     loads[1].wait()
+    loads[2].wait()
 
     def up(c):
         at = pl.ds(pl.multiple_of(c * step, step), step)
@@ -334,7 +390,7 @@
         hid[:, at] = (g / (1.0 + jnp.exp(-g)) * u).astype(BF)
 
     loop(hid.shape[1] // step, up)
-    loads[2].wait()
+    loads[3].wait()
 
     def down(d):
         to = (t + d) % n_tp
@@ -381,12 +437,12 @@
     loop(n_ep, lambda d: to_ep(d).wait_send(), 1)
 
 
-def experts(n_ep, n_tp, room, att, w_out, piece, scale, own, w_gate, w_up, w_down):
+def experts(n_ep, n_tp, room, att, w_out, pick, scale, own, w_gate, w_up, w_down, tok):
     vmem = pl.BlockSpec(memory_space=pltpu.VMEM)
     hbm = pl.BlockSpec(memory_space=pl.ANY)
     dma = pltpu.SemaphoreType.DMA
     width = w_out.shape[1]
-    total = piece.shape[0]
+    total = pick.shape[0]
     part, share = att.shape[0] // n_tp, width // n_tp
     flops = 6 * total * width * w_gate.shape[1] + 2 * att.shape[0] * att.shape[1] * width
     return pl.pallas_call(
@@ -395,12 +451,14 @@
             jax.ShapeDtypeStruct((part, width), BF),
             jax.ShapeDtypeStruct((own.shape[0], share), BF),
         ),
-        in_specs=[vmem] * 5 + [hbm] * 3,
+        in_specs=[vmem] * 5 + [hbm] * 4,
         out_specs=(vmem, vmem),
         scratch_shapes=[
             pltpu.VMEM(w_gate.shape, BF),
             pltpu.VMEM(w_up.shape, BF),
             pltpu.VMEM(w_down.shape, BF),
+            pltpu.VMEM(tok.shape, BF),
+            pltpu.VMEM((total, width), BF),
             pltpu.VMEM((total, w_gate.shape[1]), BF),
             pltpu.VMEM((n_tp, part, width), BF),
             pltpu.VMEM((n_tp, part, width), BF),
@@ -408,7 +466,7 @@
             pltpu.VMEM((n_tp, total, share), BF),
             pltpu.VMEM((n_ep, room, share), BF),
             pltpu.VMEM((n_ep, room, share), BF),
-            dma((3,)),
+            dma((4,)),
             dma((n_tp,)),
             dma((n_tp,)),
             dma((n_tp,)),
@@ -423,13 +481,7 @@
             flops=flops, bytes_accessed=20 * 1024 * 1024, transcendentals=0
         ),
         name="experts",
-    )(att, w_out, piece, scale, own, w_gate, w_up, w_down)
-
-
-def lay_heads(weights, heads, width, offset):
-    depth = weights.shape[0]
-    split = weights.reshape(depth, heads, width)
-    return jnp.pad(split, ((0, 0), (0, 0), (offset, LANES - width - offset)))
+    )(att, w_out, pick, scale, own, w_gate, w_up, w_down, tok)
 
 
 def shards(
@@ -490,26 +542,26 @@
     )
     sent_b = jnp.concatenate([rms_rows(tok_part, norm_gain_b), extra], axis=1)
 
-    q_normed = rms_rows(q_latent, q_gain)
-    w_nope = lay_heads(w_q_nope, heads, NOPE, 0)
-    w_rope = lay_heads(w_q_rope, heads, ROPE, NOPE)
-    turn = w_q_rope.reshape(-1, heads, ROPE)
-    turned = jnp.concatenate([-turn[..., half:], turn[..., :half]], axis=-1)
-    w_turned = jnp.pad(turned, ((0, 0), (0, 0), (NOPE, LANES - NOPE - ROPE)))
     cos_q, sin_q = angle_tables(e_at * own_rows + jnp.arange(own_rows, dtype=jnp.int32))
     ones = jnp.ones((own_rows, NOPE), F32)
     tail = jnp.zeros((own_rows, LANES - NOPE - ROPE), F32)
     cos_row = jnp.concatenate([ones, cos_q, cos_q, tail], axis=1)
     sin_row = jnp.concatenate([0.0 * ones, sin_q, sin_q, tail], axis=1)
-    plain = jnp.einsum("rd,dhl->hrl", q_normed, w_nope + w_rope, preferred_element_type=F32)
-    swapped = jnp.einsum("rd,dhl->hrl", q_normed, w_turned, preferred_element_type=F32)
-    q = (plain * cos_row + swapped * sin_row).astype(BF)
-
-    w_keys = lay_heads(w_k_nope, heads, NOPE, 0).reshape(-1, heads * LANES)
-    w_vals = lay_heads(w_value, heads, VDIM, 0).reshape(-1, heads * LANES)
-    w_kv = jnp.concatenate([w_keys, w_vals], axis=1)
-    attended, tok_all = attention(n_ep, n_tp, sent, sent_b, q, w_kv)
-    attended = attended.transpose(1, 0, 2).reshape(own_rows, heads * VDIM)
+    attended, tok_all = attention(
+        n_ep,
+        n_tp,
+        heads,
+        sent,
+        sent_b,
+        q_latent,
+        q_gain[None, :],
+        cos_row,
+        sin_row,
+        w_q_nope,
+        w_q_rope,
+        w_k_nope,
+        w_value,
+    )
     tok_all = tok_all.reshape(n_ep * rows_b, width + LANES)
 
     room = -(-(3 * rows_b // n_ep) // 16) * 16
@@ -529,7 +581,6 @@
     chosen = index[:, None] == row[None, :]
     pick = chosen.astype(BF)
     row_weight = jnp.sum(jnp.where(chosen, weight[None, :], 0.0), axis=1, keepdims=True)
-    piece = jnp.dot(pick, tok_all[:, :width], preferred_element_type=F32).astype(BF)
     named = (routes[:, :, None] == jnp.arange(n_ep, dtype=jnp.int32)).astype(F32)
     used = jnp.sum(named, axis=1)
     ahead = jnp.dot(before.T, used.astype(BF), preferred_element_type=F32)
@@ -537,7 +588,7 @@
     own = own.astype(BF).reshape(rows_b, n_ep * room)
     scale = jnp.broadcast_to(row_weight, (n_ep * room, LANES))
     mixer_out, expert_mix = experts(
-        n_ep, n_tp, room, attended, w_out, piece, scale, own, w_gate[0], w_up[0], w_down[0]
+        n_ep, n_tp, room, attended, w_out, pick, scale, own, w_gate[0], w_up[0], w_down[0], tok_all
     )
     return (mixer_out, expert_mix)
 

time: 147 us -> 137 us (0.932)
  matrix products: 7.23 us -> 0.22 us
  local copies, waits for them, and re-layouts: 13.4 us -> 8.6 us
  other arithmetic: 11.8 us -> 13.9 us
    dot_general x3 -> x0, matrix products: 7.01 us -> none  [the longest x1 5.23 us: shards(): jnp.dot(pick, tok_all[:, :width], preferred_element_type=F32).astype(BF)]
    unnamed x18 -> x7, local copies, waits for them, and re-layouts: 6.2 us -> 3.75 us
    reduce_sum x3 -> x2, other arithmetic: 3.24 us -> 1.99 us  [rms_rows(): jnp.mean(wide * wide, axis=-1, keepdims=True) + EPSILON]
    convert_element_type x5 -> x4, other arithmetic: 3.96 us -> 3.28 us  [rms_rows(): return (scaled * gain.astype(F32)).astype(BF)]
where the time goes in v3:
time: 137 us
  Pallas kernels  113 us (82%)
  other arithmetic  13.9 us (10%)
  local copies, waits for them, and re-layouts  8.6 us (6%)
    pallas_call x1, Pallas kernels, attention(): pl.pallas_call(functools.partial(attention_kernel, heads, n_ep, n_tp), ou...  57.5 us
    pallas_call x1, Pallas kernels, experts(): pl.pallas_call(functools.partial(experts_kernel, n_ep, n_tp), out_shape=(...  55.7 us
    unnamed x7, local copies, waits for them, and re-layouts  3.75 us
    convert_element_type x4, other arithmetic, rms_rows(): return (scaled * gain.astype(F32)).astype(BF)  3.28 us

profile of v3, /device:TPU:1, one launch (start us, length us, event | category | flops | bytes accessed | tf_op | source)
XLA Modules:
  0.0 136.7 jit_solution(11120439935207331846)
XLA Ops:
  0.6 0.0 copy-start
  0.7 0.9 fusion.14
  1.6 1.0 fusion.10
  2.7 0.1 pad.7.clone
  2.8 0.7 convert_element_type.100
  3.5 0.7 constant_dynamic-slice_fusion.1
  4.2 0.8 fusion.31
  5.0 1.3 broadcast_in_dim.33.gain_ref
  6.3 0.7 convert_reduce_fusion
  7.0 0.1 fusion.25
  7.1 0.1 eq.88
  7.2 0.0 copy-done
  7.2 0.7 convert_element_type.107
  7.9 0.1 copy.45
  8.0 0.2 fusion.27
  8.2 0.1 subtract_convert_fusion
  8.3 0.1 copy.44
  8.4 0.1 copy.43
  8.5 0.3 fusion.24
  8.8 0.2 copy.42
  9.0 0.9 fusion.16
  10.0 0.8 concatenate.12.sent_ref
  10.7 1.0 fusion.12
  11.7 0.8 concatenate.13.tok_ref
  12.5 0.1 copy.41
  12.7 0.7 and_convert_fusion.own_ref
  13.3 1.0 multiply_sine_fusion
  14.3 1.1 maximum_maximum_fusion.1
  15.4 57.5 %attention.1 = (bf16[512,256]{1,0:T(8,128)(2,1)}, bf16[32,32,2176]{2,1,0:T(8,128)(2,1)}) custom-call(bf16[128,384]{1,0:T(8,128)(2,1)} %concatenate.12.sent_ref, bf16[32,2176]{1,0:T(8,128)(2,1)} %concatenate.13.tok_ref, bf16[512,512]{1,0:T(8,128)(2,1)} %lat_ref.1, bf16[1,512]{1,0:T(2,128)(2,1)} %broadcast_in_dim.33.gain_ref, ...), custom_call_target="tpu_custom_call" | custom-call | flops 8589934592 | bytes 8388608 | tf_op jit(solution)/shard_map/attention/pallas_call | solution.py:275
  72.9 1.0 slice_convert_fusion
  73.9 0.9 fusion.5
  74.8 0.2 fusion.9
  75.0 0.2 fusion.13
  75.3 0.1 fusion.2
  75.4 0.3 select_reduce_fusion
  75.7 0.8 broadcast_in_dim.39.scale_ref
  76.5 1.1 fusion.pick_ref
  77.6 55.7 %experts.1 = (bf16[128,2048]{1,0:T(8,128)(2,1)}, bf16[128,512]{1,0:T(8,128)(2,1)}) custom-call(bf16[512,256]{1,0:T(8,128)(2,1)} %get-tuple-element.4.att_ref, bf16[256,2048]{1,0:T(8,128)(2,1)} %wo_ref.1, bf16[384,1024]{1,0:T(8,128)(2,1)} %fusion.pick_ref, f32[384,128]{1,0:T(8,128)} %broadcast_in_dim.39.scale_ref, bf16[128,384]{1,0:T(8,128)(2,1)} %and_convert_fusion.own_ref, ...), custom_call_target="tpu_custom_call" | custom-call | flops 5368709120 | bytes 20971520 | tf_op jit(solution)/shard_map/experts/pallas_call | solution.py:448
  133.3 1.9 %copy.49 = bf16[128,2048]{1,0:T(8,128)(2,1)} copy(bf16[128,2048]{1,0:T(8,128)(2,1)} %get-tuple-element.21) | data formatting | bytes 1048576
  135.2 1.6 %copy.50 = bf16[128,512]{1,0:T(8,128)(2,1)} copy(bf16[128,512]{1,0:T(8,128)(2,1)} %get-tuple-element.22) | data formatting | bytes 262144
  (21 shorter events, 0.2 us)
Async XLA Ops:
  0.6 6.5 %copy-start = (bf16[512,32]{0,1:T(8,128)(2,1)S(1)}, bf16[512,32]{0,1:T(8,128)(2,1)}, u32[]{:S(2)}) copy-start(bf16[512,32]{0,1:T(8,128)(2,1)} %param.19) | copy-start | bytes 98308

commit v4 on v3

--- a/solution.py
+++ b/solution.py
@@ -56,6 +56,8 @@
     def __init__(self, n_ep, n_tp, own, buf, local, recv, send_z, send_t, send_c):
         self.n_tp, self.nz = n_tp, n_ep // 2
         self.own, self.buf, self.local = own, buf, local
+        self.square = n_tp == 4
+        self.direct = 3 if self.square else n_tp
         self.recv, self.send_z, self.send_t, self.send_c = recv, send_z, send_t, send_c
         ep = lax.axis_index("ep")
         self.z, self.core, self.t = ep // 2, ep % 2, lax.axis_index("tp")
@@ -67,8 +69,10 @@
     def at_z(self, d):
         return (self.z + self.nz - d) % self.nz
 
-    def at_t(self, d):
-        return (self.t + self.n_tp - d) % self.n_tp
+    def at_t(self, d, back=True):
+        if self.square:
+            return (self.t // 2 + d // 2) % 2 * 2 + (self.t % 2 + d % 2) % 2
+        return (self.t + (self.n_tp - d if back else d)) % self.n_tp
 
     def copy_z(self, d):
         me = self.slot(self.z, self.core, self.t)
@@ -79,9 +83,16 @@
 
     def copy_t(self, dz, d):
         s = self.slot(self.at_z(dz), self.core, self.t)
-        to = (self.t + d) % self.n_tp
+        to = self.at_t(d, False)
         return remote(
             self.buf.at[s], self.buf.at[s], self.send_t.at[dz * self.n_tp + d], self.recv.at[s], self.ep, to
+        )
+
+    def relay(self, dz):
+        s = self.slot(self.at_z(dz), self.core, self.at_t(1 + dz % 2))
+        to = self.at_t(2 - dz % 2)
+        return remote(
+            self.buf.at[s], self.buf.at[s], self.send_t.at[dz * self.n_tp + 3], self.recv.at[s], self.ep, to
         )
 
     def copy_c(self, dz, d):
@@ -111,7 +122,7 @@
             def _():
                 self.landed(self.slot(self.at_z(dz), self.core, self.t))
 
-            loop(self.n_tp, lambda d: self.copy_t(dz, d).start(), 1)
+            loop(self.direct, lambda d: self.copy_t(dz, d).start(), 1)
             self.copy_c(dz, 0).start()
 
         loop(self.nz, one)
@@ -122,9 +133,19 @@
                 self.landed(self.slot(self.at_z(dz), self.core, self.at_t(d)))
                 self.copy_c(dz, d).start()
 
-            loop(self.n_tp, inner, 1)
+            loop(self.direct, inner, 1)
+            if self.square:
+                self.relay(dz).start()
 
         loop(self.nz, one)
+
+    def last(self):
+        def one(dz):
+            self.landed(self.slot(self.at_z(dz), self.core, self.at_t(3)))
+            self.copy_c(dz, 3).start()
+
+        if self.square:
+            loop(self.nz, one)
 
     def finish(self):
         def one(dz):
@@ -133,7 +154,9 @@
                 self.copy_c(dz, d).wait_send()
 
             loop(self.n_tp, inner)
-            loop(self.n_tp, lambda d: self.copy_t(dz, d).wait_send(), 1)
+            loop(self.direct, lambda d: self.copy_t(dz, d).wait_send(), 1)
+            if self.square:
+                self.relay(dz).wait_send()
 
         loop(self.nz, one)
         loop(self.nz, lambda d: self.copy_z(d).wait_send(), 1)
@@ -213,6 +236,7 @@
         q = q + jnp.dot(normed, turned, preferred_element_type=F32) * sin_ref[...]
         q_ref[h] = q.astype(BF)
     latents.to_sibling()
+    latents.last()
     latents.finish()
     tokens.over_tp()
     group = max(1, 512 // part)
@@ -253,8 +277,12 @@
         done = [attend_head(h, here) for h in range(heads)]
         out_ref[here, :] = done[0] if heads == 1 else jnp.concatenate(done, axis=1)
 
+        @pl.when(step == max(rows // q_block // 2 - 1, 0))
+        def _():
+            tokens.to_sibling()
+
     loop(rows // q_block, attend)
-    tokens.to_sibling()
+    tokens.last()
     tokens.finish()
 
 

time: 137 us -> 134 us (0.978)
  Pallas kernels: 113 us -> 110 us
    pallas_call x1, Pallas kernels: 57.5 us -> 53.1 us  [attention(): pl.pallas_call(functools.partial(attention_kernel, heads, n_ep, n_tp), ou...]
    pallas_call x1, Pallas kernels: 55.7 us -> 57.3 us  [experts(): pl.pallas_call(functools.partial(experts_kernel, n_ep, n_tp), out_shape=(...]
where the time goes in v4:
time: 134 us
  Pallas kernels  110 us (82%)
  other arithmetic  13.9 us (10%)
  local copies, waits for them, and re-layouts  8.6 us (6%)
    pallas_call x1, Pallas kernels, experts(): pl.pallas_call(functools.partial(experts_kernel, n_ep, n_tp), out_shape=(...  57.3 us
    pallas_call x1, Pallas kernels, attention(): pl.pallas_call(functools.partial(attention_kernel, heads, n_ep, n_tp), ou...  53.1 us
    unnamed x7, local copies, waits for them, and re-layouts  3.75 us
    convert_element_type x4, other arithmetic, rms_rows(): return (scaled * gain.astype(F32)).astype(BF)  3.28 us

profile of v4, /device:TPU:1, one launch (start us, length us, event | category | flops | bytes accessed | tf_op | source)
XLA Modules:
  0.0 134.0 jit_solution(7104668325805554683)
XLA Ops:
  0.6 0.0 copy-start
  0.7 0.9 fusion.14
  1.6 1.0 fusion.10
  2.7 0.1 pad.7.clone
  2.8 0.7 convert_element_type.100
  3.5 0.7 constant_dynamic-slice_fusion.1
  4.2 0.8 fusion.31
  5.0 1.3 broadcast_in_dim.33.gain_ref
  6.3 0.7 convert_reduce_fusion
  7.0 0.1 fusion.25
  7.1 0.1 eq.88
  7.2 0.0 copy-done
  7.2 0.7 convert_element_type.107
  7.9 0.1 copy.45
  8.0 0.2 fusion.27
  8.2 0.1 subtract_convert_fusion
  8.3 0.1 copy.44
  8.4 0.1 copy.43
  8.5 0.3 fusion.24
  8.8 0.2 copy.42
  9.0 0.9 fusion.16
  10.0 0.8 concatenate.12.sent_ref
  10.7 1.0 fusion.12
  11.7 0.8 concatenate.13.tok_ref
  12.5 0.1 copy.41
  12.7 0.7 and_convert_fusion.own_ref
  13.3 1.0 multiply_sine_fusion
  14.3 1.1 maximum_maximum_fusion.1
  15.4 53.1 %attention.1 = (bf16[512,256]{1,0:T(8,128)(2,1)}, bf16[32,32,2176]{2,1,0:T(8,128)(2,1)}) custom-call(bf16[128,384]{1,0:T(8,128)(2,1)} %concatenate.12.sent_ref, bf16[32,2176]{1,0:T(8,128)(2,1)} %concatenate.13.tok_ref, bf16[512,512]{1,0:T(8,128)(2,1)} %lat_ref.1, bf16[1,512]{1,0:T(2,128)(2,1)} %broadcast_in_dim.33.gain_ref, ...), custom_call_target="tpu_custom_call" | custom-call | flops 8589934592 | bytes 8388608 | tf_op jit(solution)/shard_map/attention/pallas_call | solution.py:303
  68.5 1.0 slice_convert_fusion
  69.5 0.9 fusion.5
  70.4 0.2 fusion.9
  70.6 0.2 fusion.13
  70.9 0.1 fusion.2
  71.0 0.3 select_reduce_fusion
  71.3 0.8 broadcast_in_dim.39.scale_ref
  72.1 1.1 fusion.pick_ref
  73.2 57.3 %experts.1 = (bf16[128,2048]{1,0:T(8,128)(2,1)}, bf16[128,512]{1,0:T(8,128)(2,1)}) custom-call(bf16[512,256]{1,0:T(8,128)(2,1)} %get-tuple-element.4.att_ref, bf16[256,2048]{1,0:T(8,128)(2,1)} %wo_ref.1, bf16[384,1024]{1,0:T(8,128)(2,1)} %fusion.pick_ref, f32[384,128]{1,0:T(8,128)} %broadcast_in_dim.39.scale_ref, bf16[128,384]{1,0:T(8,128)(2,1)} %and_convert_fusion.own_ref, ...), custom_call_target="tpu_custom_call" | custom-call | flops 5368709120 | bytes 20971520 | tf_op jit(solution)/shard_map/experts/pallas_call | solution.py:476
  130.5 1.9 %copy.49 = bf16[128,2048]{1,0:T(8,128)(2,1)} copy(bf16[128,2048]{1,0:T(8,128)(2,1)} %get-tuple-element.21) | data formatting | bytes 1048576
  132.4 1.6 %copy.50 = bf16[128,512]{1,0:T(8,128)(2,1)} copy(bf16[128,512]{1,0:T(8,128)(2,1)} %get-tuple-element.22) | data formatting | bytes 262144
  (21 shorter events, 0.2 us)
Async XLA Ops:
  0.6 6.5 %copy-start = (bf16[512,32]{0,1:T(8,128)(2,1)S(1)}, bf16[512,32]{0,1:T(8,128)(2,1)}, u32[]{:S(2)}) copy-start(bf16[512,32]{0,1:T(8,128)(2,1)} %param.19) | copy-start | bytes 98308
